TPU v7x, 512 devices: a whole 4x8x8 slice. The times are simulated.
512 devices in a mesh: sp: 128 (over z, y, core), tp: 4 (over x).
Axes of the slice: x: 4, y: 8, z: 8, core: 2. Of those that a mesh axis runs over, the one named last changes fastest.
Arguments:
- tokens: bfloat16 [32768, 2048], P(('sp', 'tp')), may hold values from -6 to 6
- pre_gain: float32 [2048], replicated, may hold values from 0.1 to 1.9
- w_query_ret: bfloat16 [2048, 768], P('sp', 'tp'), may hold values from -0.125 to 0.125
- w_key_ret: bfloat16 [2048, 768], P('sp', 'tp'), may hold values from -0.125 to 0.125
- w_value_ret: bfloat16 [2048, 768], P('sp', 'tp'), may hold values from -0.125 to 0.125
- w_query_att: bfloat16 [2048, 768], P('sp', 'tp'), may hold values from -0.5 to 0.5
- w_key_att: bfloat16 [2048, 256], P('sp', 'tp'), may hold values from -0.125 to 0.125
- w_value_att: bfloat16 [2048, 256], P('sp', 'tp'), may hold values from -0.125 to 0.125
- w_out_ret: bfloat16 [768, 2048], P('tp', 'sp'), may hold values from -0.15625 to 0.15625
- w_out_att: bfloat16 [768, 2048], P('tp', 'sp'), may hold values from -0.15625 to 0.15625
- retain_log: float32 [32768, 12], P('sp', 'tp')
- forget_total: float32 [12, 32768], P('tp'), as said below
Outputs:
- mixed: bfloat16 [32768, 2048], P(('sp', 'tp'))
Inputs may be any that keep to these rules, and one draw needn't show every extreme that they name: `forget_total`: never rises along positions.
All inputs are finite; a program needn't handle non-finite values.
Results may differ from a plain program's by a relative error of at most 0.019.
Values may be sent and summed in bfloat16 or wider, within the bound.
A program may use at most 64 MiB of HBM per device.

v0:
```python
import functools

import jax
import jax.numpy as jnp
from jax import lax
from jax.experimental import pallas as pl
from jax.experimental.pallas import tpu as pltpu
from jax.sharding import Mesh
from jax.sharding import PartitionSpec as P

HEAD = 64
SPAN = 256
SP = ("sp_0", "sp_1", "sp_2")
SP_TP = ("sp_0", "sp_1", "sp_2", "tp")
LOG2E = 1.4426950408889634
BY_NAME = pl.DeviceIdType.MESH

EPS = 1e-06
THETA = 10000.0

DELTAS = (0, 1, -1, 2, -2, 3, -3, 4)


def ring_plan():
    slots, count = {}, 0
    for j in range(1, 8):
        slots["first", j] = count
        count += 1
    for j in range(8):
        right = 4 if j % 2 == 0 else 3
        for step in range(right):
            slots["right", j, step] = count
            count += 1
        for step in range(7 - right):
            slots["left", j, step] = count
            count += 1
    return slots, count


SLOTS, N_SLOTS = ring_plan()
SUB_OF = {delta: j for j, delta in enumerate(DELTAS)}


class SpGather:
    def __init__(self, piece, bytes_of, send_sem, recv_sem, swap_send, swap_recv):
        self.piece, self.bytes_of = piece, bytes_of
        self.send_sem, self.recv_sem = send_sem, recv_sem
        self.swap_send, self.swap_recv = swap_send, swap_recv
        self.z, self.y, self.c = (lax.axis_index(a) for a in SP)

    def block(self, half, first, second):
        z, y = (second, first) if half == 0 else (first, second)
        return z * 16 + y * 2 + self.c

    def coords(self, half):
        return (self.y, self.z) if half == 0 else (self.z, self.y)

    def axes(self, half):
        return ("sp_1", "sp_0") if half == 0 else ("sp_0", "sp_1")

    def send(self, half, block, axis, by, slot):
        here = lax.axis_index(axis)
        ref = self.piece(half, block)
        pltpu.make_async_remote_copy(
            src_ref=ref,
            dst_ref=ref,
            send_sem=self.send_sem.at[half],
            recv_sem=self.recv_sem.at[half, slot],
            device_id={axis: lax.rem(here + by + 8, 8)},
            device_id_type=BY_NAME,
        ).start()

    def swap(self, half, block):
        ref = self.piece(half, block)
        pltpu.make_async_remote_copy(
            src_ref=ref,
            dst_ref=ref,
            send_sem=self.swap_send.at[half],
            recv_sem=self.swap_recv.at[half],
            device_id={"sp_2": 1 - self.c},
            device_id_type=BY_NAME,
        ).start()

    def arrived(self, half, block, slot):
        ref = self.piece(half, block)
        pltpu.make_async_copy(ref, ref, self.recv_sem.at[half, slot]).wait()

    def greet(self):
        barrier = pltpu.get_barrier_semaphore()
        for axis in ("sp_0", "sp_1"):
            for by in (1, 7):
                pl.semaphore_signal(
                    barrier,
                    inc=1,
                    device_id={axis: lax.rem(lax.axis_index(axis) + by, 8)},
                    device_id_type=BY_NAME,
                )
        pl.semaphore_signal(
            barrier, inc=1, device_id={"sp_2": 1 - self.c}, device_id_type=BY_NAME
        )
        pl.semaphore_wait(barrier, 5)

    def round(self, r):
        for half in (0, 1):
            a, b = self.coords(half)
            first, second = self.axes(half)
            if r == 0:
                own = self.block(half, a, b)
                self.send(half, own, first, 1, SLOTS["first", SUB_OF[1]])
                self.send(half, own, first, -1, SLOTS["first", SUB_OF[-1]])
            for delta in (r, -r) if 1 <= r <= 4 else ():
                if delta not in SUB_OF:
                    continue
                block = self.block(half, lax.rem(a - delta + 8, 8), b)
                self.arrived(half, block, SLOTS["first", SUB_OF[delta]])
                step = 1 if delta > 0 else -1
                if delta + step in SUB_OF:
                    self.send(half, block, first, step, SLOTS["first", SUB_OF[delta + step]])
            if r < 8:
                block = self.block(half, lax.rem(a - DELTAS[r] + 8, 8), b)
                self.send(half, block, second, 1, SLOTS["right", r, 0])
                self.send(half, block, second, -1, SLOTS["left", r, 0])
                self.swap(half, block)
            for step in range(4):
                j = r - 1 - step
                if not 0 <= j < 8:
                    continue
                source = lax.rem(a - DELTAS[j] + 8, 8)
                for way, by in (("right", 1), ("left", -1)):
                    if (way, j, step) not in SLOTS:
                        continue
                    block = self.block(half, source, lax.rem(b - by * (step + 1) + 8, 8))
                    self.arrived(half, block, SLOTS[way, j, step])
                    if (way, j, step + 1) in SLOTS:
                        self.send(half, block, second, by, SLOTS[way, j, step + 1])
                    self.swap(half, block)

    def finish(self):
        for half in (0, 1):
            swapped, sent = self.bytes_of(half, 64), self.bytes_of(half, 63)
            pltpu.make_async_copy(swapped, swapped, self.swap_recv.at[half]).wait()
            pltpu.make_async_copy(swapped, swapped, self.swap_send.at[half]).wait()
            pltpu.make_async_copy(sent, sent, self.send_sem.at[half]).wait()


GATHER_SEMS = [
    pltpu.SemaphoreType.DMA((2,)),
    pltpu.SemaphoreType.DMA((2, N_SLOTS)),
    pltpu.SemaphoreType.DMA((2,)),
    pltpu.SemaphoreType.DMA((2,)),
    pltpu.SemaphoreType.DMA,
]
ROUNDS = 12


def gather_kernel(shard_ref, out_ref, send_sem, recv_sem, swap_send, swap_recv, local_sem):
    rows, cols = shard_ref.shape
    if rows > cols:
        piece = lambda half, b: out_ref.at[b, pl.ds(half * (rows // 2), rows // 2)]
        many = lambda half, n: out_ref.at[pl.ds(0, n), pl.ds(half * (rows // 2), rows // 2)]
    else:
        piece = lambda half, b: out_ref.at[b, :, pl.ds(half * (cols // 2), cols // 2)]
        many = lambda half, n: out_ref.at[pl.ds(0, n), :, pl.ds(half * (cols // 2), cols // 2)]
    ring = SpGather(piece, many, send_sem, recv_sem, swap_send, swap_recv)
    own = ring.z * 16 + ring.y * 2 + ring.c
    copy = pltpu.make_async_copy(shard_ref, out_ref.at[own], local_sem)
    copy.start()
    ring.greet()
    copy.wait()
    for r in range(ROUNDS):
        ring.round(r)
    ring.finish()


def sp_gather(shard, collective_id):
    rows, cols = shard.shape
    return pl.pallas_call(
        gather_kernel,
        out_shape=jax.ShapeDtypeStruct((128, rows, cols), shard.dtype),
        in_specs=[pl.BlockSpec(memory_space=pltpu.VMEM)],
        out_specs=pl.BlockSpec(memory_space=pltpu.VMEM),
        scratch_shapes=GATHER_SEMS,
        compiler_params=pltpu.CompilerParams(
            collective_id=collective_id, has_side_effects=True, vmem_limit_bytes=40 * 2**20
        ),
    )(shard).reshape(128 * rows, cols)


def attend_kernel(q_ref, gate_rows_ref, gate_keys_ref, kv_ref, out_ref, acc, tot):
    z, y, c = (lax.axis_index(a) for a in SP)
    mine = z * 16 + y * 2 + c
    acc[...] = jnp.zeros_like(acc)
    tot[...] = jnp.zeros_like(tot)

    def weigh(block, masked):
        keys = kv_ref[pl.ds(pl.multiple_of(block * SPAN, SPAN), SPAN), :]
        for h in range(3):
            rows = pl.ds(h * SPAN, SPAN)
            scores = lax.dot_general(
                q_ref[rows, :], keys, (((1,), (1,)), ((), ())), preferred_element_type=jnp.float32
            )
            fall = gate_keys_ref[pl.ds(block, 1), h, :]
            logits = scores + (gate_rows_ref[rows, :] - fall)
            if masked:
                t = lax.broadcasted_iota(jnp.int32, logits.shape, 0)
                s = lax.broadcasted_iota(jnp.int32, logits.shape, 1)
                logits = jnp.where(s <= t, logits, -jnp.inf)
            weights = jnp.exp2(logits)
            tot[rows, :] += weights[:, :128] + weights[:, 128:]
            acc[rows, :] += jnp.dot(
                weights.astype(jnp.bfloat16), keys, preferred_element_type=jnp.float32
            )

    def pair(i, carry):
        weigh(2 * i, False)
        weigh(2 * i + 1, False)
        return carry

    lax.fori_loop(0, mine // 2, pair, 0)

    @pl.when(lax.rem(mine, 2) == 1)
    def _():
        weigh(mine - 1, False)

    weigh(mine, True)
    for h in range(3):
        rows = pl.ds(h * SPAN, SPAN)
        total = jnp.sum(tot[rows, :], axis=1, keepdims=True)
        out_ref[:, h * HEAD : (h + 1) * HEAD] = (acc[rows, HEAD:] / total).astype(jnp.bfloat16)


def attend(q, gate_rows, gate_keys, kv):
    return pl.pallas_call(
        attend_kernel,
        out_shape=jax.ShapeDtypeStruct((SPAN, 3 * HEAD), jnp.bfloat16),
        in_specs=[pl.BlockSpec(memory_space=pltpu.VMEM)] * 4,
        out_specs=pl.BlockSpec(memory_space=pltpu.VMEM),
        scratch_shapes=[
            pltpu.VMEM((3 * SPAN, 128), jnp.float32),
            pltpu.VMEM((3 * SPAN, 128), jnp.float32),
        ],
        compiler_params=pltpu.CompilerParams(vmem_limit_bytes=40 * 2**20),
    )(q, gate_rows, gate_keys, kv)


def from_everyone(shard, axis):
    copies = jnp.broadcast_to(shard, (lax.axis_size(axis), *shard.shape))
    return lax.all_to_all(copies, axis, split_axis=0, concat_axis=0, tiled=True)


def in_order(parts, dim):
    lengths = list(parts.shape[1:])
    lengths[dim] *= parts.shape[0]
    return jnp.moveaxis(parts, 0, dim).reshape(lengths)


def gathered_copies(shard, axis, dim):
    parts = from_everyone(shard, axis)
    return in_order(parts, dim)


def filled_with(shard, identity):
    return jax.tree.map(
        lambda part, zero: jnp.zeros_like(part) + jnp.asarray(zero, part.dtype), shard, identity
    )


def carried_in(shard, axes, combine, identity):
    before = start = filled_with(shard, identity)
    subtotal = shard
    for axis in reversed(axes):
        devices, here = (lax.axis_size(axis), lax.axis_index(axis))
        pieces = jax.tree.map(
            lambda part, kind: lax.all_gather(part.astype(kind), axis),
            subtotal,
            (jnp.bfloat16, jnp.bfloat16),
        )
        inside, subtotal = (start, start)
        for k in range(devices):
            passed = k < here
            subtotal = combine(
                subtotal, jax.tree.map(lambda part, own: part[k].astype(own.dtype), pieces, shard)
            )
            inside = jax.tree.map(lambda new, old: jnp.where(passed, new, old), subtotal, inside)
        before = combine(inside, before)
    return before


def cut_along(shard, dim, devices):
    lengths = shard.shape
    parts = shard.reshape(*lengths[:dim], devices, lengths[dim] // devices, *lengths[dim + 1 :])
    return jnp.moveaxis(parts, dim, 0)


def sent_and_summed(shard, axis, dim):
    devices = lax.axis_size(axis)
    parts = lax.all_to_all(cut_along(shard, dim, devices), axis, 0, 0, tiled=True)
    return jnp.sum(parts.astype(jnp.float32), axis=0)


def rotate(field, positions):
    half = field.shape[-1] // 2
    inverse = THETA ** (-jnp.arange(half, dtype=jnp.float32) / half)
    angles = positions[:, None] * inverse[None, :]
    cosine = jnp.cos(angles)[:, None, :]
    sine = jnp.sin(angles)[:, None, :]
    first_half = field[..., :half]
    second_half = field[..., half:]
    return jnp.concatenate(
        [first_half * cosine - second_half * sine, first_half * sine + second_half * cosine],
        axis=-1,
    )


def head_norm(values):
    centre = jnp.mean(values, axis=-1, keepdims=True)
    spread = jnp.mean(jnp.square(values - centre), axis=-1, keepdims=True)
    return (values - centre) * lax.rsqrt(spread + EPS)


def advance(state, pair):
    decay, update = pair
    return (jnp.exp(decay)[:, None, None] * state + update, state)


def body(
    tokens,
    pre_gain,
    w_query_ret,
    w_key_ret,
    w_value_ret,
    w_query_att,
    w_key_att,
    w_value_att,
    w_out_ret,
    w_out_att,
    retain_log,
    forget_total,
):
    rows = tokens.astype(jnp.float32)
    normed = (
        rows * lax.rsqrt(jnp.mean(rows * rows, axis=-1, keepdims=True) + EPS) * pre_gain
    ).astype(jnp.bfloat16)
    gathered = gathered_copies(normed, "tp", 0)
    tok_dev = gathered.shape[0]
    offset = lax.axis_index(SP) * tok_dev
    query_places = offset + jnp.arange(tok_dev, dtype=jnp.int32)
    positions = query_places.astype(jnp.float32)

    def blocked(values):
        return values.reshape((tok_dev // SPAN, SPAN) + values.shape[1:])

    matrices = sp_gather(
        jnp.concatenate(
            (
                w_query_ret,
                w_key_ret,
                w_value_ret,
                w_query_att,
                w_key_att,
                w_value_att,
                w_out_ret.T,
                w_out_att.T,
            ),
            axis=1,
        ),
        1,
    )
    flat = jnp.dot(gathered, matrices[:, :896], preferred_element_type=jnp.float32)
    projected = tuple(
        flat[:, a:b] for a, b in ((0, 192), (192, 384), (384, 576), (576, 768), (768, 896))
    )
    heads = retain_log.shape[1]
    shape = (tok_dev, heads, HEAD)
    query = blocked(
        (rotate(projected[0].reshape(shape), positions) * HEAD ** (-0.5)).astype(jnp.bfloat16)
    )
    key_rows = blocked(rotate(projected[1].reshape(shape), positions).astype(jnp.bfloat16))
    value_rows = blocked(projected[2].astype(jnp.bfloat16).reshape(shape))
    within = jnp.cumsum(blocked(retain_log), axis=1)
    causal = jnp.arange(SPAN)[:, None] >= jnp.arange(SPAN)[None, :]
    scores = jnp.einsum("bthd,bshd->bhts", query, key_rows, preferred_element_type=jnp.float32)
    turned = jnp.transpose(within, (0, 2, 1))
    gap = jnp.where(causal, turned[:, :, :, None] - turned[:, :, None, :], 0.0)
    weights = jnp.where(causal, scores * jnp.exp(gap), 0.0).astype(jnp.bfloat16)
    local = jnp.einsum("bhts,bshd->bthd", weights, value_rows, preferred_element_type=jnp.float32)
    last = within[:, -1]
    faded = (key_rows.astype(jnp.float32) * jnp.exp(last[:, None, :] - within)[..., None]).astype(
        jnp.bfloat16
    )
    updates = jnp.einsum("bshd,bshe->bhde", faded, value_rows, preferred_element_type=jnp.float32)
    zero_state = jnp.zeros((heads, HEAD, HEAD), jnp.float32)
    final, _ = lax.scan(advance, zero_state, (last, updates))
    decay_total = jnp.sum(last, axis=0)
    own_state = final.reshape(heads, HEAD * HEAD)

    def combine(earlier, later):
        return (earlier[0] + later[0], jnp.exp(later[0])[:, None] * earlier[1] + later[1])

    identity = (jnp.zeros_like(decay_total), jnp.zeros_like(own_state))
    incoming = carried_in((decay_total, own_state), SP, combine, identity)[1]
    _, befores = lax.scan(advance, incoming.reshape(heads, HEAD, HEAD), (last, updates))
    lifted = (query.astype(jnp.float32) * jnp.exp(within)[..., None]).astype(jnp.bfloat16)
    carried = jnp.einsum(
        "bthd,bhde->bthe", lifted, befores.astype(jnp.bfloat16), preferred_element_type=jnp.float32
    )
    retained = (
        head_norm((local + carried).reshape(shape))
        .astype(jnp.bfloat16)
        .reshape(tok_dev, heads * HEAD)
    )
    kv = sp_gather(projected[4].astype(jnp.bfloat16), 2)
    query = (projected[3] * (HEAD ** (-0.5) * LOG2E)).astype(jnp.bfloat16)
    query = query.reshape(tok_dev, 3, HEAD).transpose(1, 0, 2).reshape(3 * tok_dev, HEAD)
    query = jnp.pad(query, ((0, 0), (0, HEAD)))
    gates = forget_total * LOG2E
    gate_rows = lax.dynamic_slice_in_dim(gates, offset, tok_dev, 1).reshape(3 * tok_dev, 1)
    gate_keys = gates.reshape(3, 128, SPAN).transpose(1, 0, 2)
    attended = attend(query, gate_rows, gate_keys, kv)
    wide = jnp.concatenate((retained, attended), axis=1)
    mixed = sent_and_summed(
        lax.dot_general(
            wide, matrices[:, 896:], (((1,), (1,)), ((), ())), preferred_element_type=jnp.float32
        ).astype(jnp.bfloat16),
        "tp",
        0,
    )
    return mixed.astype(jnp.bfloat16)


def solution(mesh):
    finer = Mesh(mesh.devices.reshape(8, 8, 2, mesh.shape["tp"]), ("sp_0", "sp_1", "sp_2", "tp"))
    placed = (
        P(SP_TP, None),
        P(),
        P(SP, "tp"),
        P(SP, "tp"),
        P(SP, "tp"),
        P(SP, "tp"),
        P(SP, "tp"),
        P(SP, "tp"),
        P("tp", SP),
        P("tp", SP),
        P(SP, "tp"),
        P("tp", None),
    )
    return jax.shard_map(
        body, mesh=finer, in_specs=placed, out_specs=P(SP_TP, None), check_vma=False
    )
```

profile of v0, /device:TPU:504, one launch (start us, length us, event | category | flops | bytes accessed | tf_op | source)
XLA Modules:
  0.0 269.9 jit_solution(13127283219696735593)
XLA Ops:
  0.1 1.1 fusion.9
  1.2 1.1 fusion.11
  2.3 1.1 broadcast_in_dim.18
  3.5 4.3 %all-to-all-start = ((bf16[4,64,2048]{2,1,0:T(8,128)(2,1)}), bf16[4,64,2048]{2,1,0:T(8,128)(2,1)S(1)}, u32[]{:S(2)}, u32[]{:S(2)}) async-start(bf16[4,64,2048]{2,1,0:T(8,128)(2,1)} %broadcast_in_dim.18), calls=%async_computation | async-start | bytes 2097152 | tf_op jit(solution)/shard_map/all_to_all | solution.py:248
  7.8 0.7 reshape.784
  8.5 0.9 reduce-window.6
  10.0 1.8 all-gather
  11.9 14.1 %all-gather.1 = bf16[8,1,3]{2,1,0:T(2,128)(2,1)S(1)} all-gather(bf16[1,1,3]{2,1,0:T(2,128)(2,1)S(1)} %get-tuple-element.83), channel_id=1, replica_groups=mesh['sp_0'=8,'sp_1'=8,'sp_2'=2,'tp'=4] {'sp_1'}, dimensions={0}, use_global_device_ids=true | all-gather | bytes 54 | tf_op jit(solution)/shard_map/all_gather | solution.py:274
  27.1 13.0 %all-gather.2 = bf16[8,1,3]{2,1,0:T(2,128)(2,1)S(1)} all-gather(bf16[1,1,3]{2,1,0:T(2,128)(2,1)S(1)} %get-tuple-element.72), channel_id=1, replica_groups=mesh['sp_0'=8,'sp_1'=8,'sp_2'=2,'tp'=4] {'sp_0'}, dimensions={0}, use_global_device_ids=true | all-gather | bytes 54 | tf_op jit(solution)/shard_map/all_gather | solution.py:274
  40.8 42.7 %shard_map.118 = bf16[128,16,1280]{2,1,0:T(8,128)(2,1)S(1)} custom-call(bf16[16,1280]{1,0:T(8,128)(2,1)S(1)} %concatenate.21.shard_ref), custom_call_target="tpu_custom_call" | custom-call | tf_op jit(solution)/shard_map/pallas_call | solution.py:177
  83.6 2.3 copy-done
  85.9 0.6 fusion.48
  86.5 0.6 bitcast_add_fusion.1
  87.3 3.3 %fusion.78 = (bf16[256,896]{1,0:T(8,128)(2,1)S(1)}, f32[256,896]{1,0:T(8,128)S(1)}) fusion(bf16[256,2048]{1,0:T(8,128)(2,1)S(1)} %bitcast.195, bf16[2048,1280]{1,0:T(8,128)(2,1)} %bitcast.191), kind=kOutput, calls=%fused_computation.169 | convolution fusion | flops 939753472 | bytes 6094848 | tf_op jit(solution)/shard_map/dot_general | solution.py:369
  91.6 1.9 all_gather.27
  93.8 24.9 %all_gather.28 = bf16[8,3,4096]{2,1,0:T(4,128)(2,1)S(1)} all-gather(bf16[1,3,4096]{2,1,0:T(4,128)(2,1)S(1)} %add_convert_fusion.3), channel_id=1, replica_groups=mesh['sp_0'=8,'sp_1'=8,'sp_2'=2,'tp'=4] {'sp_1'}, dimensions={0}, use_global_device_ids=true | all-gather | bytes 221184 | tf_op jit(solution)/shard_map/all_gather | solution.py:274
  119.0 24.8 %all_gather.29 = bf16[8,3,4096]{2,1,0:T(4,128)(2,1)S(1)} all-gather(bf16[1,3,4096]{2,1,0:T(4,128)(2,1)S(1)} %add_convert_fusion.2), channel_id=1, replica_groups=mesh['sp_0'=8,'sp_1'=8,'sp_2'=2,'tp'=4] {'sp_0'}, dimensions={0}, use_global_device_ids=true | all-gather | bytes 221184 | tf_op jit(solution)/shard_map/all_gather | solution.py:274
  145.7 1.4 fusion.5
  147.1 1.4 bitcast_reduce_fusion
  149.2 44.6 %shard_map.119 = bf16[128,256,128]{2,1,0:T(8,128)(2,1)S(1)} custom-call(bf16[256,128]{1,0:T(8,128)(2,1)S(1)} %slice.267.shard_ref), custom_call_target="tpu_custom_call" | custom-call | tf_op jit(solution)/shard_map/pallas_call | solution.py:177
  193.9 52.1 %shard_map.120 = bf16[256,192]{1,0:T(8,128)(2,1)S(1)} custom-call(bf16[768,128]{1,0:T(8,128)(2,1)S(1)} %pad.4.q_ref, f32[768,1]{1,0:T(8,128)S(1)} %bitcast.194, f32[128,3,256]{2,1,0:T(4,128)S(1)} %bitcast.193, bf16[32768,128]{1,0:T(8,128)(2,1)S(1)} %bitcast.190), custom_call_target="tpu_custom_call" | custom-call | tf_op jit(solution)/shard_map/pallas_call | solution.py:233
  246.0 2.2 convolution_convert_fusion
  248.2 20.8 %all_to_all.10 = bf16[4,64,2048]{2,1,0:T(8,128)(2,1)S(1)} all-to-all(bf16[4,64,2048]{2,1,0:T(8,128)(2,1)S(1)} %bitcast.196), channel_id=1, replica_groups=mesh['sp_0'=8,'sp_1'=8,'sp_2'=2,'tp'=4] {'tp'}, dimensions={0} | all-to-all | bytes 2097152 | tf_op jit(solution)/shard_map/all_to_all | solution.py:297
  268.9 0.9 reduce_sum.46
  (114 shorter events, 6.6 us)
Async XLA Ops:
  0.0 40.3 %copy-start.1 = (f32[3,32768]{1,0:T(4,128)S(1)}, f32[3,32768]{1,0:T(4,128)}, u32[]{:S(2)}) copy-start(f32[3,32768]{1,0:T(4,128)} %param.23) | copy-start | bytes 1179652
  0.0 40.6 %copy-start.10 = (bf16[192,16]{0,1:T(8,128)(2,1)S(1)}, bf16[192,16]{0,1:T(8,128)(2,1)}, u32[]{:S(2)}) copy-start(bf16[192,16]{0,1:T(8,128)(2,1)} %param.21) | copy-start | bytes 18436
  0.0 40.7 %copy-start.9 = (bf16[192,16]{0,1:T(8,128)(2,1)S(1)}, bf16[192,16]{0,1:T(8,128)(2,1)}, u32[]{:S(2)}) copy-start(bf16[192,16]{0,1:T(8,128)(2,1)} %param.20) | copy-start | bytes 18436
  0.0 40.7 %copy-start.19 = (bf16[16,64]{1,0:T(8,128)(2,1)S(1)}, bf16[16,64]{1,0:T(8,128)(2,1)}, u32[]{:S(2)}) copy-start(bf16[16,64]{1,0:T(8,128)(2,1)} %param.19) | copy-start | bytes 6148
  0.0 40.7 %copy-start.18 = (bf16[16,64]{1,0:T(8,128)(2,1)S(1)}, bf16[16,64]{1,0:T(8,128)(2,1)}, u32[]{:S(2)}) copy-start(bf16[16,64]{1,0:T(8,128)(2,1)} %param.18) | copy-start | bytes 6148
  0.0 40.7 %copy-start.8 = (bf16[16,192]{1,0:T(8,128)(2,1)S(1)}, bf16[16,192]{1,0:T(8,128)(2,1)}, u32[]{:S(2)}) copy-start(bf16[16,192]{1,0:T(8,128)(2,1)} %param.17) | copy-start | bytes 18436
  0.0 40.7 %copy-start.7 = (bf16[16,192]{1,0:T(8,128)(2,1)S(1)}, bf16[16,192]{1,0:T(8,128)(2,1)}, u32[]{:S(2)}) copy-start(bf16[16,192]{1,0:T(8,128)(2,1)} %param.16) | copy-start | bytes 18436
  0.0 40.7 %copy-start.6 = (bf16[16,192]{1,0:T(8,128)(2,1)S(1)}, bf16[16,192]{1,0:T(8,128)(2,1)}, u32[]{:S(2)}) copy-start(bf16[16,192]{1,0:T(8,128)(2,1)} %param.15) | copy-start | bytes 18436
  0.1 40.7 %copy-start.5 = (bf16[16,192]{1,0:T(8,128)(2,1)S(1)}, bf16[16,192]{1,0:T(8,128)(2,1)}, u32[]{:S(2)}) copy-start(bf16[16,192]{1,0:T(8,128)(2,1)} %param.14) | copy-start | bytes 18436
  3.5 83.8 %all-to-all-start = ((bf16[4,64,2048]{2,1,0:T(8,128)(2,1)}), bf16[4,64,2048]{2,1,0:T(8,128)(2,1)S(1)}, u32[]{:S(2)}, u32[]{:S(2)}) async-start(bf16[4,64,2048]{2,1,0:T(8,128)(2,1)} %broadcast_in_dim.18), calls=%async_computation | async-start | bytes 2097152 | tf_op jit(solution)/shard_map/all_to_all | solution.py:248
  26.0 92.8 %copy-start.15 = (f32[3]{0:T(128)}, f32[3]{0:T(128)S(1)}, u32[]{:S(2)}) copy-start(f32[3]{0:T(128)S(1)} %get-tuple-element.78) | copy-start | bytes 40
  26.0 92.8 %copy-start.16 = (f32[3]{0:T(128)}, f32[3]{0:T(128)S(1)}, u32[]{:S(2)}) copy-start(f32[3]{0:T(128)S(1)} %get-tuple-element.79) | copy-start | bytes 40
  26.0 92.8 %copy-start.17 = (f32[3]{0:T(128)}, f32[3]{0:T(128)S(1)}, u32[]{:S(2)}) copy-start(f32[3]{0:T(128)S(1)} %get-tuple-element.80) | copy-start | bytes 40
  27.1 91.7 %copy-start.11 = (f32[3]{0:T(128)}, f32[3]{0:T(128)S(1)}, u32[]{:S(2)}) copy-start(f32[3]{0:T(128)S(1)} %get-tuple-element.74) | copy-start | bytes 40
  27.1 91.7 %copy-start.12 = (f32[3]{0:T(128)}, f32[3]{0:T(128)S(1)}, u32[]{:S(2)}) copy-start(f32[3]{0:T(128)S(1)} %get-tuple-element.75) | copy-start | bytes 40
  27.1 91.7 %copy-start.13 = (f32[3]{0:T(128)}, f32[3]{0:T(128)S(1)}, u32[]{:S(2)}) copy-start(f32[3]{0:T(128)S(1)} %get-tuple-element.76) | copy-start | bytes 40
  27.1 91.7 %copy-start.14 = (f32[3]{0:T(128)}, f32[3]{0:T(128)S(1)}, u32[]{:S(2)}) copy-start(f32[3]{0:T(128)S(1)} %get-tuple-element.77) | copy-start | bytes 40
  83.6 2.3 copy-start
  91.1 27.9 %copy-start.2 = (bf16[256,192]{0,1:T(8,128)(2,1)}, bf16[256,192]{0,1:T(8,128)(2,1)S(1)}, u32[]{:S(2)}) copy-start(bf16[256,192]{0,1:T(8,128)(2,1)S(1)} %copy.70) | copy-start | bytes 294916
  91.2 27.7 %copy-start.3 = (bf16[256,3,32]{0,2,1:T(8,128)(2,1)}, bf16[256,3,32]{0,2,1:T(8,128)(2,1)S(1)}, u32[]{:S(2)}) copy-start(bf16[256,3,32]{0,2,1:T(8,128)(2,1)S(1)} %get-tuple-element.62) | copy-start | bytes 147460
  91.3 27.7 %copy-start.4 = (bf16[256,3,32]{0,2,1:T(8,128)(2,1)}, bf16[256,3,32]{0,2,1:T(8,128)(2,1)S(1)}, u32[]{:S(2)}) copy-start(bf16[256,3,32]{0,2,1:T(8,128)(2,1)S(1)} %get-tuple-element.63) | copy-start | bytes 147460
where the time goes:
time: 270 us
  Pallas kernels  139 us (51%)
  blocking collectives  101 us (37%)
  local copies, waits for them, and re-layouts  8.94 us (3%)
  matrix products  8.36 us (3%)
  other arithmetic  6.91 us (3%)
  starting transfers between devices  4.29 us (2%)
    pallas_call x2, Pallas kernels, sp_gather(): pl.pallas_call(gather_kernel, out_shape=jax.ShapeDtypeStruct((128, rows,...  87.4 us
    all_gather x6, blocking collectives, carried_in(): lax.all_gather(part.astype(kind), axis)  80.5 us
    pallas_call x1, Pallas kernels, attend(): pl.pallas_call(attend_kernel, out_shape=jax.ShapeDtypeStruct((SPAN, 3 * H...  52.1 us
    all_to_all x1, blocking collectives, sent_and_summed(): lax.all_to_all(cut_along(shard, dim, devices), axis, 0, 0, tiled=True)  20.8 us
  transfers between devices with their start and end apart: 1, of which 0 were waited for; matrix products, arithmetic and copies ran while one was open for 2% of the time, Pallas kernels for 16%

commit v1 on v0

v1 whole, which is shorter than its diff:
```python
import jax
import jax.numpy as jnp
from jax import lax
from jax.experimental import pallas as pl
from jax.experimental.pallas import tpu as pltpu
from jax.sharding import Mesh
from jax.sharding import PartitionSpec as P

HEAD = 64
SPAN = 256
SP = ("sp_0", "sp_1", "sp_2")
SP_TP = ("sp_0", "sp_1", "sp_2", "tp")
LOG2E = 1.4426950408889634
BY_NAME = pl.DeviceIdType.MESH

EPS = 1e-06
THETA = 10000.0

DELTAS = (0, 1, -1, 2, -2, 3, -3, 4)


def ring_plan():
    slots, count = {}, 0
    for j in range(1, 8):
        slots["first", j] = count
        count += 1
    for j in range(8):
        right = 4 if j % 2 == 0 else 3
        for step in range(right):
            slots["right", j, step] = count
            count += 1
        for step in range(7 - right):
            slots["left", j, step] = count
            count += 1
    return slots, count


SLOTS, N_SLOTS = ring_plan()
SUB_OF = {delta: j for j, delta in enumerate(DELTAS)}


class SpGather:
    def __init__(self, piece, bytes_of, send_sem, recv_sem, swap_send, swap_recv):
        self.piece, self.bytes_of = piece, bytes_of
        self.send_sem, self.recv_sem = send_sem, recv_sem
        self.swap_send, self.swap_recv = swap_send, swap_recv
        self.z, self.y, self.c = (lax.axis_index(a) for a in SP)

    def block(self, half, first, second):
        z, y = (second, first) if half == 0 else (first, second)
        return z * 16 + y * 2 + self.c

    def coords(self, half):
        return (self.y, self.z) if half == 0 else (self.z, self.y)

    def axes(self, half):
        return ("sp_1", "sp_0") if half == 0 else ("sp_0", "sp_1")

    def send(self, half, block, axis, by, slot):
        here = lax.axis_index(axis)
        ref = self.piece(half, block)
        pltpu.make_async_remote_copy(
            src_ref=ref,
            dst_ref=ref,
            send_sem=self.send_sem.at[half],
            recv_sem=self.recv_sem.at[half, slot],
            device_id={axis: lax.rem(here + by + 8, 8)},
            device_id_type=BY_NAME,
        ).start()

    def swap(self, half, block):
        ref = self.piece(half, block)
        pltpu.make_async_remote_copy(
            src_ref=ref,
            dst_ref=ref,
            send_sem=self.swap_send.at[half],
            recv_sem=self.swap_recv.at[half],
            device_id={"sp_2": 1 - self.c},
            device_id_type=BY_NAME,
        ).start()

    def arrived(self, half, block, slot):
        ref = self.piece(half, block)
        pltpu.make_async_copy(ref, ref, self.recv_sem.at[half, slot]).wait()

    def round(self, r):
        for half in (0, 1):
            a, b = self.coords(half)
            first, second = self.axes(half)
            if r == 0:
                own = self.block(half, a, b)
                self.send(half, own, first, 1, SLOTS["first", SUB_OF[1]])
                self.send(half, own, first, -1, SLOTS["first", SUB_OF[-1]])
            for delta in (r, -r) if 1 <= r <= 4 else ():
                if delta not in SUB_OF:
                    continue
                block = self.block(half, lax.rem(a - delta + 8, 8), b)
                self.arrived(half, block, SLOTS["first", SUB_OF[delta]])
                step = 1 if delta > 0 else -1
                if delta + step in SUB_OF:
                    self.send(half, block, first, step, SLOTS["first", SUB_OF[delta + step]])
            if r < 8:
                block = self.block(half, lax.rem(a - DELTAS[r] + 8, 8), b)
                self.send(half, block, second, 1, SLOTS["right", r, 0])
                self.send(half, block, second, -1, SLOTS["left", r, 0])
                self.swap(half, block)
            for step in range(4):
                j = r - 2 - 2 * step
                if not 0 <= j < 8:
                    continue
                source = lax.rem(a - DELTAS[j] + 8, 8)
                for way, by in (("right", 1), ("left", -1)):
                    if (way, j, step) not in SLOTS:
                        continue
                    block = self.block(half, source, lax.rem(b - by * (step + 1) + 8, 8))
                    self.arrived(half, block, SLOTS[way, j, step])
                    if (way, j, step + 1) in SLOTS:
                        self.send(half, block, second, by, SLOTS[way, j, step + 1])
                    self.swap(half, block)

    def finish(self):
        for half in (0, 1):
            swapped, sent = self.bytes_of(half, 64), self.bytes_of(half, 63)
            pltpu.make_async_copy(swapped, swapped, self.swap_recv.at[half]).wait()
            pltpu.make_async_copy(swapped, swapped, self.swap_send.at[half]).wait()
            pltpu.make_async_copy(sent, sent, self.send_sem.at[half]).wait()


def greet(*axes):
    barrier = pltpu.get_barrier_semaphore()
    count = 0
    for axis in axes:
        size = lax.axis_size(axis)
        for by in (1, size - 1) if size > 2 else (1,):
            pl.semaphore_signal(
                barrier,
                inc=1,
                device_id={axis: lax.rem(lax.axis_index(axis) + by, size)},
                device_id_type=BY_NAME,
            )
            count += 1
    pl.semaphore_wait(barrier, count)


def remote(src, dst, send_sem, recv_sem, axis, by):
    size = lax.axis_size(axis)
    return pltpu.make_async_remote_copy(
        src_ref=src,
        dst_ref=dst,
        send_sem=send_sem,
        recv_sem=recv_sem,
        device_id={axis: lax.rem(lax.axis_index(axis) + by + size, size)},
        device_id_type=BY_NAME,
    )


def wait_for(ref, sem):
    pltpu.make_async_copy(ref, ref, sem).wait()


GATHER_SEMS = [
    pltpu.SemaphoreType.DMA((2,)),
    pltpu.SemaphoreType.DMA((2, N_SLOTS)),
    pltpu.SemaphoreType.DMA((2,)),
    pltpu.SemaphoreType.DMA((2,)),
]
ROUNDS = 16
VMEM = pl.BlockSpec(memory_space=pltpu.VMEM)
IN_WIDTH = 896
ALL_WIDTH = 1280
WIDE = 3 * HEAD


def running_totals(logs):
    t = lax.broadcasted_iota(jnp.int32, (SPAN, SPAN), 0)
    s = lax.broadcasted_iota(jnp.int32, (SPAN, SPAN), 1)
    below = jnp.where(s <= t, 1.0, 0.0).astype(jnp.float32)
    dims = (((0,), (1,)), ((), ()))
    columns = jnp.dot(
        below, logs, preferred_element_type=jnp.float32, precision=lax.Precision.HIGHEST
    )
    rows = lax.dot_general(
        logs, below, dims, preferred_element_type=jnp.float32, precision=lax.Precision.HIGHEST
    )
    return columns, rows


def per_head(columns):
    rows = columns.shape[0]
    return jnp.concatenate(
        [jnp.broadcast_to(columns[:, h : h + 1], (rows, HEAD)) for h in range(3)], axis=1
    )


def project_kernel(
    tokens_ref,
    gain_ref,
    wqr_ref,
    wkr_ref,
    wvr_ref,
    wqa_ref,
    wka_ref,
    wva_ref,
    wor_ref,
    woa_ref,
    cos_ref,
    sin_ref,
    logs_ref,
    wall_ref,
    qr_ref,
    kr_ref,
    vr_ref,
    qa_ref,
    kv_ref,
    update_ref,
    total_ref,
    x_ref,
    send_sem,
    recv_sem,
    swap_send,
    swap_recv,
    x_send,
    x_recv,
):
    half_width = ALL_WIDTH // 2
    ring = SpGather(
        lambda half, b: wall_ref.at[b, :, pl.ds(half * half_width, half_width)],
        lambda half, n: wall_ref.at[pl.ds(0, n), :, pl.ds(half * half_width, half_width)],
        send_sem,
        recv_sem,
        swap_send,
        swap_recv,
    )
    own = ring.z * 16 + ring.y * 2 + ring.c
    x = lax.axis_index("tp")
    at = 0
    for ref in (wqr_ref, wkr_ref, wvr_ref, wqa_ref, wka_ref, wva_ref):
        wall_ref[own, :, at : at + ref.shape[1]] = ref[...]
        at += ref.shape[1]
    for ref in (wor_ref, woa_ref):
        wall_ref[own, :, at : at + WIDE] = ref[...].astype(jnp.float32).T.astype(jnp.bfloat16)
        at += WIDE
    rows = tokens_ref[...].astype(jnp.float32)
    x_ref[x] = (
        rows * lax.rsqrt(jnp.mean(rows * rows, axis=-1, keepdims=True) + EPS) * gain_ref[...]
    ).astype(jnp.bfloat16)
    greet("sp_0", "sp_1", "sp_2", "tp")
    ring.round(0)

    def part(slot, k):
        return x_ref.at[lax.rem(slot + 4, 4), :, pl.ds(k * 1024, 1024)]

    def pass_on(slot, k, by, sem):
        remote(part(slot, k), part(slot, k), x_send, x_recv.at[sem], "tp", by).start()

    pass_on(x, 0, 1, 0)
    pass_on(x, 1, -1, 1)
    pass_on(x, 1, 1, 2)
    pass_on(x, 0, -1, 3)
    ring.round(1)
    columns, _ = running_totals(logs_ref[...])
    last = columns[SPAN - 1 : SPAN]
    fade = jnp.exp(per_head(last - columns))
    total_ref[...] = jnp.broadcast_to(per_head(last), (8, WIDE))
    ring.round(2)
    ring.round(3)
    wait_for(part(x - 1, 0), x_recv.at[0])
    pass_on(x - 1, 0, 1, 4)
    wait_for(part(x + 1, 1), x_recv.at[1])
    pass_on(x + 1, 1, -1, 5)
    for r in range(4, ROUNDS):
        ring.round(r)
    wait_for(part(x - 1, 1), x_recv.at[2])
    wait_for(part(x + 1, 0), x_recv.at[3])
    wait_for(part(x - 2, 0), x_recv.at[4])
    wait_for(part(x + 2, 1), x_recv.at[5])
    ring.finish()
    sent = x_ref.at[pl.ds(0, 3)]
    wait_for(sent, x_send)

    flat = jnp.dot(
        x_ref[...].reshape(SPAN, 2048),
        wall_ref[:, :, :IN_WIDTH].reshape(2048, IN_WIDTH),
        preferred_element_type=jnp.float32,
    )
    both = flat[:, : 2 * WIDE]
    lane = lax.rem(lax.broadcasted_iota(jnp.int32, both.shape, 1), HEAD)
    turned = jnp.where(
        lane < HEAD // 2, pltpu.roll(both, 2 * WIDE - HEAD // 2, 1), pltpu.roll(both, HEAD // 2, 1)
    )
    cosine = jnp.concatenate([cos_ref[...]] * 3, axis=1)
    sine = jnp.concatenate([sin_ref[...]] * 3, axis=1)
    roped = both * cosine + turned * sine
    qr_ref[...] = (roped[:, :WIDE] * HEAD**-0.5).astype(jnp.bfloat16)
    key = roped[:, WIDE:].astype(jnp.bfloat16)
    kr_ref[...] = key
    value = flat[:, 2 * WIDE : 3 * WIDE].astype(jnp.bfloat16)
    vr_ref[...] = value
    faded = (key.astype(jnp.float32) * fade).astype(jnp.bfloat16)
    for h in range(3):
        lanes = slice(h * HEAD, (h + 1) * HEAD)
        update_ref[:, lanes] = lax.dot_general(
            faded[:, lanes],
            value[:, lanes],
            (((0,), (0,)), ((), ())),
            preferred_element_type=jnp.float32,
        )
        query = flat[:, 3 * WIDE + h * HEAD : 3 * WIDE + (h + 1) * HEAD] * (HEAD**-0.5 * LOG2E)
        qa_ref[h * SPAN : (h + 1) * SPAN, :] = jnp.concatenate(
            [query, jnp.zeros_like(query)], axis=1
        ).astype(jnp.bfloat16)
    kv_ref[...] = flat[:, 4 * WIDE :].astype(jnp.bfloat16)


def project(*operands):
    bf16 = jnp.bfloat16
    square = jax.ShapeDtypeStruct((SPAN, WIDE), bf16)
    return pl.pallas_call(
        project_kernel,
        out_shape=(
            jax.ShapeDtypeStruct((128, 16, ALL_WIDTH), bf16),
            square,
            square,
            square,
            jax.ShapeDtypeStruct((3 * SPAN, 128), bf16),
            jax.ShapeDtypeStruct((SPAN, 128), bf16),
            jax.ShapeDtypeStruct((HEAD, WIDE), jnp.float32),
            jax.ShapeDtypeStruct((8, WIDE), jnp.float32),
        ),
        in_specs=[VMEM] * len(operands),
        out_specs=(VMEM,) * 8,
        scratch_shapes=[
            pltpu.VMEM((4, 64, 2048), bf16),
            *GATHER_SEMS,
            pltpu.SemaphoreType.DMA,
            pltpu.SemaphoreType.DMA((6,)),
        ],
        compiler_params=pltpu.CompilerParams(
            collective_id=1, has_side_effects=True, vmem_limit_bytes=40 * 2**20
        ),
    )(*operands)


class Prefix:
    def __init__(self, states, decays, sems):
        self.states, self.decays = states, decays
        self.state_send, self.state_recv, self.decay_send, self.decay_recv = sems
        self.z, self.y, self.c = (lax.axis_index(a) for a in SP)

    def send(self, slot, axis, by, sem):
        for ref, out, arrive in (
            (self.states, self.state_send, self.state_recv),
            (self.decays, self.decay_send, self.decay_recv),
        ):
            remote(ref.at[slot], ref.at[slot], out, arrive.at[sem], axis, by).start()

    def wait(self, slot, sem):
        wait_for(self.states.at[slot], self.state_recv.at[sem])
        wait_for(self.decays.at[slot], self.decay_recv.at[sem])

    def store(self, slot, pair):
        self.states[slot] = pair[0].astype(jnp.bfloat16)
        self.decays[slot] = pair[1]

    def load(self, slot):
        return self.states[slot].astype(jnp.float32), self.decays[slot]

    @staticmethod
    def join(earlier, later):
        return jnp.exp(later[1][:1]) * earlier[0] + later[0], earlier[1] + later[1]

    @staticmethod
    def keep(flag, pair):
        return jnp.where(flag, pair[0], 0.0), jnp.where(flag, pair[1], 0.0)

    def ring_hop(self, hop, base, here, axis, first_sem):
        if hop == 0:
            self.send(base + here, axis, 1, first_sem)
            self.send(base + here, axis, -1, first_sem + 4)
            return
        right = base + lax.rem(here - hop + 8, 8)
        self.wait(right, first_sem + hop - 1)
        if hop < 4:
            self.send(right, axis, 1, first_sem + hop)
            left = base + lax.rem(here + hop, 8)
            self.wait(left, first_sem + 4 + hop - 1)
            if hop < 3:
                self.send(left, axis, -1, first_sem + 4 + hop)

    def round(self, r):
        if r == 0:
            self.send(self.c, "sp_2", 1, 0)
        if r == 1:
            self.wait(1 - self.c, 0)
            self.store(2 + self.y, self.join(self.load(0), self.load(1)))
            self.ring_hop(0, 2, self.y, "sp_1", 1)
        if r in (3, 5, 7, 9):
            self.ring_hop((r - 1) // 2, 2, self.y, "sp_1", 1)
        if r == 9:
            total = self.load(2)
            for k in range(1, 8):
                total = self.join(total, self.load(2 + k))
            self.store(10 + self.z, total)
            self.ring_hop(0, 10, self.z, "sp_0", 8)
        if r in (11, 13, 15, 17):
            self.ring_hop((r - 9) // 2, 10, self.z, "sp_0", 8)

    def finish(self):
        before = self.keep(0 < self.z, self.load(10))
        for k in range(1, 7):
            before = self.keep_if(k < self.z, before, self.load(10 + k))
        for k in range(7):
            before = self.keep_if(k < self.y, before, self.load(2 + k))
        before = self.keep_if(self.c == 1, before, self.load(0))
        for ref, sem in ((self.states, self.state_send), (self.decays, self.decay_send)):
            wait_for(ref.at[pl.ds(0, 15)], sem)
        return before[0]

    def keep_if(self, flag, before, later):
        return self.join(before, self.keep(flag, later))


PREFIX_SEMS = [
    pltpu.SemaphoreType.DMA,
    pltpu.SemaphoreType.DMA((15,)),
    pltpu.SemaphoreType.DMA,
    pltpu.SemaphoreType.DMA((15,)),
]


def exchange_kernel(
    kv_ref,
    update_ref,
    total_ref,
    kvs_ref,
    before_ref,
    states,
    decays,
    local_sem,
    send_sem,
    recv_sem,
    swap_send,
    swap_recv,
    *prefix_sems,
):
    rows = SPAN // 2
    ring = SpGather(
        lambda half, b: kvs_ref.at[b, pl.ds(half * rows, rows)],
        lambda half, n: kvs_ref.at[pl.ds(0, n), pl.ds(half * rows, rows)],
        send_sem,
        recv_sem,
        swap_send,
        swap_recv,
    )
    prefix = Prefix(states, decays, prefix_sems)
    own = ring.z * 16 + ring.y * 2 + ring.c
    copy = pltpu.make_async_copy(kv_ref, kvs_ref.at[own], local_sem)
    copy.start()
    prefix.store(ring.c, (update_ref[...], total_ref[...]))
    greet(*SP)
    copy.wait()
    for r in range(18):
        prefix.round(r)
        if r < ROUNDS:
            ring.round(r)
    before_ref[...] = prefix.finish().astype(jnp.bfloat16)
    ring.finish()


def exchange(kv, update, total):
    return pl.pallas_call(
        exchange_kernel,
        out_shape=(
            jax.ShapeDtypeStruct((128, SPAN, 128), jnp.bfloat16),
            jax.ShapeDtypeStruct((HEAD, WIDE), jnp.bfloat16),
        ),
        in_specs=[VMEM] * 3,
        out_specs=(VMEM,) * 2,
        scratch_shapes=[
            pltpu.VMEM((18, HEAD, WIDE), jnp.bfloat16),
            pltpu.VMEM((18, 8, WIDE), jnp.float32),
            pltpu.SemaphoreType.DMA,
            *GATHER_SEMS,
            *PREFIX_SEMS,
        ],
        compiler_params=pltpu.CompilerParams(
            collective_id=2, has_side_effects=True, vmem_limit_bytes=40 * 2**20
        ),
    )(kv, update, total)


def retain(qr_ref, kr_ref, vr_ref, logs, before, out_ref):
    columns, rows = running_totals(logs)
    t = lax.broadcasted_iota(jnp.int32, (SPAN, SPAN), 0)
    s = lax.broadcasted_iota(jnp.int32, (SPAN, SPAN), 1)
    causal = s <= t
    lifted = (qr_ref[...].astype(jnp.float32) * jnp.exp(per_head(columns))).astype(jnp.bfloat16)
    for h in range(3):
        lanes = slice(h * HEAD, (h + 1) * HEAD)
        scores = lax.dot_general(
            qr_ref[:, lanes],
            kr_ref[:, lanes],
            (((1,), (1,)), ((), ())),
            preferred_element_type=jnp.float32,
        )
        gap = jnp.where(causal, columns[:, h : h + 1] - rows[h : h + 1, :], 0.0)
        weights = jnp.where(causal, scores * jnp.exp(gap), 0.0).astype(jnp.bfloat16)
        raw = jnp.dot(weights, vr_ref[:, lanes], preferred_element_type=jnp.float32)
        raw += jnp.dot(lifted[:, lanes], before[:, lanes], preferred_element_type=jnp.float32)
        raw -= jnp.mean(raw, axis=-1, keepdims=True)
        spread = jnp.mean(raw * raw, axis=-1, keepdims=True)
        out_ref[:, lanes] = (raw * lax.rsqrt(spread + EPS)).astype(jnp.bfloat16)


def mix_kernel(
    qr_ref, kr_ref, vr_ref, logs_ref, before_ref, qa_ref, gates_ref, kvs_ref, wall_ref,
    out_ref, acc, tot, wide
):
    z, y, c = (lax.axis_index(a) for a in SP)
    mine = z * 16 + y * 2 + c
    retain(qr_ref, kr_ref, vr_ref, logs_ref[...], before_ref[...], wide)
    acc[...] = jnp.zeros_like(acc)
    tot[...] = jnp.zeros_like(tot)

    def gate_row(block, h):
        span = pl.ds(pl.multiple_of(block * SPAN, SPAN), SPAN)
        return gates_ref[h : h + 1, span] * LOG2E

    gate_columns = jnp.transpose(
        jnp.concatenate(
            [gate_row(mine, h) for h in range(3)] + [jnp.zeros((5, SPAN), jnp.float32)], axis=0
        )
    )

    def weigh(block, masked):
        keys = kvs_ref[block]
        for h in range(3):
            rows = pl.ds(h * SPAN, SPAN)
            scores = lax.dot_general(
                qa_ref[rows, :], keys, (((1,), (1,)), ((), ())), preferred_element_type=jnp.float32
            )
            logits = scores + (gate_columns[:, h : h + 1] - gate_row(block, h))
            if masked:
                t = lax.broadcasted_iota(jnp.int32, logits.shape, 0)
                s = lax.broadcasted_iota(jnp.int32, logits.shape, 1)
                logits = jnp.where(s <= t, logits, -jnp.inf)
            weights = jnp.exp2(logits)
            tot[rows, :] += weights[:, :128] + weights[:, 128:]
            acc[rows, :] += jnp.dot(
                weights.astype(jnp.bfloat16), keys, preferred_element_type=jnp.float32
            )

    def pair(i, carry):
        weigh(2 * i, False)
        weigh(2 * i + 1, False)
        return carry

    lax.fori_loop(0, mine // 2, pair, 0)

    @pl.when(lax.rem(mine, 2) == 1)
    def _():
        weigh(mine - 1, False)

    weigh(mine, True)
    for h in range(3):
        rows = pl.ds(h * SPAN, SPAN)
        total = jnp.sum(tot[rows, :], axis=1, keepdims=True)
        wide[:, WIDE + h * HEAD : WIDE + (h + 1) * HEAD] = (acc[rows, HEAD:] / total).astype(
            jnp.bfloat16
        )
    for k in range(4):
        columns = wall_ref[k * 32 : (k + 1) * 32, :, IN_WIDTH:].reshape(512, 2 * WIDE)
        out_ref[:, k * 512 : (k + 1) * 512] = lax.dot_general(
            wide[...], columns, (((1,), (1,)), ((), ())), preferred_element_type=jnp.float32
        ).astype(jnp.bfloat16)


def mix(*operands):
    return pl.pallas_call(
        mix_kernel,
        out_shape=jax.ShapeDtypeStruct((SPAN, 2048), jnp.bfloat16),
        in_specs=[VMEM] * len(operands),
        out_specs=VMEM,
        scratch_shapes=[
            pltpu.VMEM((3 * SPAN, 128), jnp.float32),
            pltpu.VMEM((3 * SPAN, 128), jnp.float32),
            pltpu.VMEM((SPAN, 2 * WIDE), jnp.bfloat16),
        ],
        compiler_params=pltpu.CompilerParams(vmem_limit_bytes=40 * 2**20),
    )(*operands)


def cut_along(shard, dim, devices):
    lengths = shard.shape
    parts = shard.reshape(*lengths[:dim], devices, lengths[dim] // devices, *lengths[dim + 1 :])
    return jnp.moveaxis(parts, dim, 0)


def sent_and_summed(shard, axis, dim):
    devices = lax.axis_size(axis)
    parts = lax.all_to_all(cut_along(shard, dim, devices), axis, 0, 0, tiled=True)
    return jnp.sum(parts.astype(jnp.float32), axis=0)


def angles_of(positions):
    half = HEAD // 2
    inverse = THETA ** (-jnp.arange(half, dtype=jnp.float32) / half)
    return positions[:, None] * inverse[None, :]


def body(
    tokens,
    pre_gain,
    w_query_ret,
    w_key_ret,
    w_value_ret,
    w_query_att,
    w_key_att,
    w_value_att,
    w_out_ret,
    w_out_att,
    retain_log,
    forget_total,
):
    offset = lax.axis_index(SP) * SPAN
    positions = (offset + jnp.arange(SPAN, dtype=jnp.int32)).astype(jnp.float32)
    angles = angles_of(positions)
    cosine, sine = jnp.cos(angles), jnp.sin(angles)
    cosine = jnp.concatenate([cosine] * 4, axis=1)
    sine = jnp.concatenate([-sine, sine] * 2, axis=1)
    wall, qr, kr, vr, qa, kv, update, total = project(
        tokens,
        pre_gain.reshape(1, -1),
        w_query_ret,
        w_key_ret,
        w_value_ret,
        w_query_att,
        w_key_att,
        w_value_att,
        w_out_ret,
        w_out_att,
        cosine,
        sine,
        retain_log,
    )
    kvs, before = exchange(kv, update, total)
    partial = mix(qr, kr, vr, retain_log, before, qa, forget_total, kvs, wall)
    return sent_and_summed(partial, "tp", 0).astype(jnp.bfloat16)


def solution(mesh):
    finer = Mesh(mesh.devices.reshape(8, 8, 2, mesh.shape["tp"]), ("sp_0", "sp_1", "sp_2", "tp"))
    placed = (
        P(SP_TP, None),
        P(),
        P(SP, "tp"),
        P(SP, "tp"),
        P(SP, "tp"),
        P(SP, "tp"),
        P(SP, "tp"),
        P(SP, "tp"),
        P("tp", SP),
        P("tp", SP),
        P(SP, "tp"),
        P("tp", None),
    )
    return jax.shard_map(
        body, mesh=finer, in_specs=placed, out_specs=P(SP_TP, None), check_vma=False
    )
```

time: 270 us -> 175 us (0.65)
  blocking collectives: 101 us -> 19 us
  matrix products: 8.36 us -> 0 us
  other arithmetic: 6.91 us -> 1.74 us
  starting transfers between devices: 4.29 us -> 0 us
  local copies, waits for them, and re-layouts: 8.94 us -> 12.5 us
    all_gather x6 -> x0, blocking collectives: 80.5 us -> none  [carried_in(): lax.all_gather(part.astype(kind), axis)]
    unnamed x44 -> x23, local copies, waits for them, and re-layouts: 2.69 us -> 12.5 us
    dot_general x5 -> x0, matrix products: 8.36 us -> none  [the longest x1 3.32 us: body(): jnp.dot(gathered, matrices[:, :896], preferred_element_type=jnp.float32)]
    all_to_all x1 -> x0, starting transfers between devices: 4.29 us -> none  [from_everyone(): return lax.all_to_all(copies, axis, split_axis=0, concat_axis=0, tiled=True)]
  transfers between devices with their start and end apart: 1 -> 0, of which waited for: 0 -> 0; matrix products, arithmetic and copies ran while one was open for 2% -> 0% of each run, Pallas kernels for 16% -> 0%
where the time goes in v1:
time: 175 us; the launch traced here: 174 us
  Pallas kernels  141 us (81%)
  blocking collectives  19 us (11%)
  local copies, waits for them, and re-layouts  12.5 us (7%)
    pallas_call x1, Pallas kernels, mix(): pl.pallas_call(mix_kernel, out_shape=jax.ShapeDtypeStruct((SPAN, 2048), j...  57.7 us
    pallas_call x1, Pallas kernels, exchange(): pl.pallas_call(exchange_kernel, out_shape=(jax.ShapeDtypeStruct((128, SPA...  43.7 us
    pallas_call x1, Pallas kernels, project(): pl.pallas_call(project_kernel, out_shape=(jax.ShapeDtypeStruct((128, 16,...  39.6 us
    all_to_all x1, blocking collectives, sent_and_summed(): lax.all_to_all(cut_along(shard, dim, devices), axis, 0, 0, tiled=True)  19 us
    unnamed x23, local copies, waits for them, and re-layouts  12.5 us

profile of v1, /device:TPU:504, one launch (start us, length us, event | category | flops | bytes accessed | tf_op | source)
XLA Modules:
  0.0 174.3 jit_solution(11637040485596113602)
XLA Ops:
  0.0 0.8 copy.18.wor_ref
  0.8 0.8 copy.19.woa_ref
  1.7 0.8 copy.20.logs_ref
  2.5 0.5 fusion
  3.0 0.3 pad_maximum_fusion
  3.3 0.0 copy-start.2
  3.3 0.9 copy-done.2
  4.3 0.0 copy-start.3
  4.3 0.7 copy-done.3
  5.0 0.0 copy-start.4
  5.0 0.7 copy-done.4
  5.7 0.7 copy-done.5
  6.4 0.7 copy-done.6
  7.1 0.7 copy-done.7
  7.7 0.7 copy-done.8
  8.4 0.7 copy-done.9
  9.1 39.6 %shard_map.118 = (bf16[128,16,1280]{2,1,0:T(8,128)(2,1)S(1)}, bf16[256,192]{1,0:T(8,128)(2,1)S(1)}, bf16[256,192]{1,0:T(8,128)(2,1)S(1)}, bf16[256,192]{1,0:T(8,...) custom-call(bf16[64,2048]{1,0:T(8,128)(2,1)S(1)} %copy-done.2, ...), custom_call_target="tpu_custom_call" | custom-call | tf_op jit(solution)/shard_map/pallas_call | solution.py:318
  48.7 43.7 %shard_map.119 = (bf16[128,256,128]{2,1,0:T(8,128)(2,1)S(1)}, bf16[64,192]{1,0:T(8,128)(2,1)S(1)}) custom-call(bf16[256,128]{1,0:T(8,128)(2,1)S(1)} %get-tuple-element.18.kv_ref, f32[64,192]{1,0:T(8,128)S(1)} %get-tuple-element.19.update_ref, f32[8,192]{1,0:T(8,128)S(1)} %get-tuple-element.20.total_ref), custom_call_target="tpu_custom_call" | custom-call | tf_op jit(solution)/shard_map/pallas_call | solution.py:471
  92.4 0.0 copy-start
  92.4 3.2 %copy-done = bf16[128,256,128]{2,1,0:T(8,128)(2,1)} copy-done((bf16[128,256,128]{2,1,0:T(8,128)(2,1)}, bf16[128,256,128]{2,1,0:T(8,128)(2,1)S(1)}, u32[]{:S(2)}) %copy-start) | copy-done | bytes 8388632
  95.7 1.0 copy-done.1
  96.7 57.7 %shard_map.120 = bf16[256,2048]{1,0:T(8,128)(2,1)S(1)} custom-call(bf16[256,192]{1,0:T(8,128)(2,1)S(1)} %get-tuple-element.15.qr_ref, bf16[256,192]{1,0:T(8,128)(2,1)S(1)} %get-tuple-element.16.kr_ref, bf16[256,192]{1,0:T(8,128)(2,1)S(1)} %get-tuple-element.17.vr_ref, f32[256,3]{1,0:T(8,128)S(1)} %copy.20.logs_ref, ...), custom_call_target="tpu_custom_call" | custom-call | tf_op jit(solution)/shard_map/pallas_call | solution.py:579
  154.4 19.0 %all_to_all.5 = bf16[4,64,2048]{2,1,0:T(8,128)(2,1)S(1)} all-to-all(bf16[4,64,2048]{2,1,0:T(8,128)(2,1)S(1)} %bitcast.2), channel_id=1, replica_groups=mesh['sp_0'=8,'sp_1'=8,'sp_2'=2,'tp'=4] {'tp'}, dimensions={0} | all-to-all | bytes 2097152 | tf_op jit(solution)/shard_map/all_to_all | solution.py:601
  173.4 0.9 reduce_sum.12
  (8 shorter events, 0.0 us)
Async XLA Ops:
  3.3 1.0 copy-start.2
  4.3 0.7 copy-start.3
  5.0 0.7 copy-start.4
  5.7 0.7 copy-start.5
  6.4 0.7 copy-start.6
  7.0 0.7 copy-start.7
  7.7 0.7 copy-start.8
  8.4 0.7 copy-start.9
  92.4 3.2 %copy-start = (bf16[128,256,128]{2,1,0:T(8,128)(2,1)}, bf16[128,256,128]{2,1,0:T(8,128)(2,1)S(1)}, u32[]{:S(2)}) copy-start(bf16[128,256,128]{2,1,0:T(8,128)(2,1)S(1)} %get-tuple-element.23.kvs_ref) | copy-start | bytes 25165828
  95.7 1.0 copy-start.1

commit v2 on v1

v2 whole, which is shorter than its diff:
```python
import jax
import jax.numpy as jnp
from jax import lax
from jax.experimental import pallas as pl
from jax.experimental.pallas import tpu as pltpu
from jax.sharding import Mesh
from jax.sharding import PartitionSpec as P

HEAD = 64
SPAN = 256
SP = ("sp_0", "sp_1", "sp_2")
SP_TP = ("sp_0", "sp_1", "sp_2", "tp")
LOG2E = 1.4426950408889634
BY_NAME = pl.DeviceIdType.MESH
VMEM = pl.BlockSpec(memory_space=pltpu.VMEM)
ANY = pl.BlockSpec(memory_space=pl.ANY)
IN_WIDTH = 896
ALL_WIDTH = 1280
WIDE = 3 * HEAD

EPS = 1e-06
THETA = 10000.0

DELTAS = (0, 1, -1, 2, -2, 3, -3, 4)


def ring_plan():
    slots = {}
    for delta in DELTAS[1:]:
        slots["first", delta] = len(slots)
    for delta in DELTAS:
        right = 4 if delta <= 0 else 3
        for way, steps in ((1, right), (-1, 7 - right)):
            for step in range(steps):
                slots[way, delta, step] = len(slots)
    return slots


SLOTS = ring_plan()
STEPS = 9


def greet(*axes):
    barrier = pltpu.get_barrier_semaphore()
    count = 0
    for axis in axes:
        size = lax.axis_size(axis)
        for by in (1, size - 1) if size > 2 else (1,):
            pl.semaphore_signal(
                barrier,
                inc=1,
                device_id={axis: lax.rem(lax.axis_index(axis) + by, size)},
                device_id_type=BY_NAME,
            )
            count += 1
    return lambda: pl.semaphore_wait(barrier, count)


def remote(src, dst, send_sem, recv_sem, axis, by):
    size = lax.axis_size(axis)
    return pltpu.make_async_remote_copy(
        src_ref=src,
        dst_ref=dst,
        send_sem=send_sem,
        recv_sem=recv_sem,
        device_id={axis: lax.rem(lax.axis_index(axis) + by + size, size)},
        device_id_type=BY_NAME,
    )


def wait_for(ref, sem):
    pltpu.make_async_copy(ref, ref, sem).wait()


def ring_index(at):
    return lax.rem(at + 8, 8)


class SpGather:
    def __init__(self, ref, part, sems):
        self.ref, self.part = ref, part
        self.send_sem, self.recv_sem, self.swap_send, self.swap_recv = sems
        self.z, self.y, self.c = (lax.axis_index(a) for a in SP)

    def piece(self, half, first, second):
        z, y = (second, first) if half == 0 else (first, second)
        return self.ref.at[(z, y, self.c) + self.part(half)]

    def slab(self, half, second):
        place = (second, slice(None)) if half == 0 else (slice(None), second)
        return self.ref.at[place + (self.c,) + self.part(half)]

    def coords(self, half):
        return (self.y, self.z) if half == 0 else (self.z, self.y)

    def send(self, half, ref, axis, by, slot):
        remote(
            ref, ref, self.send_sem.at[half], self.recv_sem.at[half, SLOTS[slot]], axis, by
        ).start()

    def arrived(self, half, ref, slot):
        wait_for(ref, self.recv_sem.at[half, SLOTS[slot]])

    def swap(self, half, second):
        ref = self.slab(half, second)
        remote(ref, ref, self.swap_send.at[half], self.swap_recv.at[half], "sp_2", 1).start()

    def step(self, s):
        for half in (0, 1):
            a, b = self.coords(half)
            first, second = ("sp_1", "sp_0") if half == 0 else ("sp_0", "sp_1")
            for delta in sorted({s, -s}, reverse=True):
                if delta not in DELTAS:
                    continue
                ref = self.piece(half, ring_index(a - delta), b)
                if delta:
                    self.arrived(half, ref, ("first", delta))
                for further in (1, -1) if delta == 0 else (delta + (1 if delta > 0 else -1),):
                    if further in DELTAS:
                        self.send(half, ref, first, 1 if further > 0 else -1, ("first", further))
                for by in (1, -1):
                    self.send(half, ref, second, by, (by, delta, 0))
            if s == 4:
                self.swap(half, b)
            for k in range(4):
                for delta in DELTAS:
                    if abs(delta) != s - 1 - k:
                        continue
                    for by in (1, -1):
                        if (by, delta, k) not in SLOTS:
                            continue
                        ref = self.piece(half, ring_index(a - delta), ring_index(b - by * (k + 1)))
                        self.arrived(half, ref, (by, delta, k))
                        if (by, delta, k + 1) in SLOTS:
                            self.send(half, ref, second, by, (by, delta, k + 1))
            if 5 <= s < 8:
                self.swap(half, ring_index(b - (s - 4)))
                self.swap(half, ring_index(b + (s - 4)))
            if s == 8:
                self.swap(half, ring_index(b + 4))

    def finish(self):
        for half in (0, 1):
            core = self.ref.at[(slice(None), slice(None), 0) + self.part(half)]
            wait_for(core, self.swap_recv.at[half])
            wait_for(core, self.swap_send.at[half])
            wait_for(
                self.ref.at[(slice(0, 7), slice(None), 0) + self.part(half)],
                self.send_sem.at[half],
            )
            wait_for(
                self.ref.at[(0, slice(0, 7), 0) + self.part(half)], self.send_sem.at[half]
            )


GATHER_SEMS = [
    pltpu.SemaphoreType.DMA((2,)),
    pltpu.SemaphoreType.DMA((2, len(SLOTS))),
    pltpu.SemaphoreType.DMA((2,)),
    pltpu.SemaphoreType.DMA((2,)),
]


def running_totals(logs):
    t = lax.broadcasted_iota(jnp.int32, (SPAN, SPAN), 0)
    s = lax.broadcasted_iota(jnp.int32, (SPAN, SPAN), 1)
    below = jnp.where(s <= t, 1.0, 0.0).astype(jnp.float32)
    dims = (((1,), (1,)), ((), ()))
    exact = lax.Precision.HIGHEST
    columns = lax.dot_general(
        below, logs, dims, preferred_element_type=jnp.float32, precision=exact
    )
    rows = lax.dot_general(logs, below, dims, preferred_element_type=jnp.float32, precision=exact)
    return columns, rows


def per_head(columns):
    rows = columns.shape[0]
    return jnp.concatenate(
        [jnp.broadcast_to(columns[:, h : h + 1], (rows, HEAD)) for h in range(3)], axis=1
    )


class Prefix:
    def __init__(self, states, decays, sems):
        self.states, self.decays = states, decays
        self.state_send, self.state_recv, self.decay_send, self.decay_recv = sems
        self.z, self.y, self.c = (lax.axis_index(a) for a in SP)

    def send(self, slot, axis, by, sem):
        for ref, out, arrive in (
            (self.states, self.state_send, self.state_recv),
            (self.decays, self.decay_send, self.decay_recv),
        ):
            remote(ref.at[slot], ref.at[slot], out, arrive.at[sem], axis, by).start()

    def wait(self, slot, sem):
        wait_for(self.states.at[slot], self.state_recv.at[sem])
        wait_for(self.decays.at[slot], self.decay_recv.at[sem])

    def store(self, slot, pair):
        self.states[slot] = pair[0].astype(jnp.bfloat16)
        self.decays[slot] = pair[1]

    def load(self, slot):
        return self.states[slot].astype(jnp.float32), self.decays[slot]

    @staticmethod
    def join(earlier, later):
        return jnp.exp(later[1][:1]) * earlier[0] + later[0], earlier[1] + later[1]

    @staticmethod
    def keep(flag, pair):
        return jnp.where(flag, pair[0], 0.0), jnp.where(flag, pair[1], 0.0)

    def ring_hop(self, hop, base, here, axis, first_sem):
        if hop == 0:
            self.send(base + here, axis, 1, first_sem)
            self.send(base + here, axis, -1, first_sem + 4)
            return
        right = base + lax.rem(here - hop + 8, 8)
        self.wait(right, first_sem + hop - 1)
        if hop < 4:
            self.send(right, axis, 1, first_sem + hop)
            left = base + lax.rem(here + hop, 8)
            self.wait(left, first_sem + 4 + hop - 1)
            if hop < 3:
                self.send(left, axis, -1, first_sem + 4 + hop)

    def step(self, s):
        if s == 0:
            self.send(self.c, "sp_2", 1, 0)
        if s == 1:
            self.wait(1 - self.c, 0)
            self.store(2 + self.y, self.join(self.load(0), self.load(1)))
            self.ring_hop(0, 2, self.y, "sp_1", 1)
        if 2 <= s <= 5:
            self.ring_hop(s - 1, 2, self.y, "sp_1", 1)
        if s == 5:
            total = self.load(2)
            for k in range(1, 8):
                total = self.join(total, self.load(2 + k))
            self.store(10 + self.z, total)
            self.ring_hop(0, 10, self.z, "sp_0", 8)
        if 6 <= s <= 9:
            self.ring_hop(s - 5, 10, self.z, "sp_0", 8)

    def finish(self):
        before = self.keep(0 < self.z, self.load(10))
        for k in range(1, 7):
            before = self.keep_if(k < self.z, before, self.load(10 + k))
        for k in range(7):
            before = self.keep_if(k < self.y, before, self.load(2 + k))
        before = self.keep_if(self.c == 1, before, self.load(0))
        for ref, sem in ((self.states, self.state_send), (self.decays, self.decay_send)):
            wait_for(ref.at[pl.ds(0, 15)], sem)
        return before[0]

    def keep_if(self, flag, before, later):
        return self.join(before, self.keep(flag, later))


PREFIX_SEMS = [
    pltpu.SemaphoreType.DMA,
    pltpu.SemaphoreType.DMA((15,)),
    pltpu.SemaphoreType.DMA,
    pltpu.SemaphoreType.DMA((15,)),
]


def retain_inside(qr_ref, kr_ref, vr_ref, logs, raw_ref, lifted_ref):
    columns, rows = running_totals(logs)
    t = lax.broadcasted_iota(jnp.int32, (SPAN, SPAN), 0)
    s = lax.broadcasted_iota(jnp.int32, (SPAN, SPAN), 1)
    causal = s <= t
    lifted = qr_ref[...].astype(jnp.float32) * jnp.exp(per_head(columns))
    lifted_ref[...] = lifted.astype(jnp.bfloat16)
    for h in range(3):
        lanes = slice(h * HEAD, (h + 1) * HEAD)
        scores = lax.dot_general(
            qr_ref[:, lanes],
            kr_ref[:, lanes],
            (((1,), (1,)), ((), ())),
            preferred_element_type=jnp.float32,
        )
        gap = jnp.where(causal, columns[:, h : h + 1] - rows[h : h + 1, :], 0.0)
        weights = jnp.where(causal, scores * jnp.exp(gap), 0.0).astype(jnp.bfloat16)
        raw_ref[:, lanes] = jnp.dot(
            weights, vr_ref[:, lanes], preferred_element_type=jnp.float32
        )


def retain_earlier(raw_ref, lifted_ref, before, wide_ref):
    for h in range(3):
        lanes = slice(h * HEAD, (h + 1) * HEAD)
        raw = raw_ref[:, lanes] + jnp.dot(
            lifted_ref[:, lanes], before[:, lanes], preferred_element_type=jnp.float32
        )
        raw -= jnp.mean(raw, axis=-1, keepdims=True)
        spread = jnp.mean(raw * raw, axis=-1, keepdims=True)
        wide_ref[:, lanes] = (raw * lax.rsqrt(spread + EPS)).astype(jnp.bfloat16)


def layer_kernel(
    tokens_ref,
    gain_ref,
    wqr_ref,
    wkr_ref,
    wvr_ref,
    wqa_ref,
    wka_ref,
    wva_ref,
    wor_ref,
    woa_ref,
    cos_ref,
    sin_ref,
    logs_ref,
    gates_ref,
    out_ref,
    tokens_in,
    gain_in,
    wqr_in,
    wkr_in,
    wvr_in,
    wqa_in,
    wka_in,
    wva_in,
    wor_in,
    woa_in,
    cos_in,
    sin_in,
    logs_in,
    gates_in,
    wall_ref,
    x_ref,
    qr_ref,
    kr_ref,
    vr_ref,
    qa_ref,
    update,
    kvs,
    states,
    decays,
    acc,
    tot,
    raw,
    lifted,
    wide,
    part,
    inbox,
    load_sem,
    x_send,
    x_recv,
    out_send,
    out_recv,
    *sems,
):
    half_width = ALL_WIDTH // 2
    ring = SpGather(
        wall_ref, lambda half: (slice(None), pl.ds(half * half_width, half_width)), sems[:4]
    )
    x = lax.axis_index("tp")
    place = (ring.z, ring.y, ring.c)
    loads = [
        pltpu.make_async_copy(here, there, load_sem.at[k])
        for k, (here, there) in enumerate(
            (
                (wqr_ref, wqr_in),
                (wkr_ref, wkr_in),
                (wvr_ref, wvr_in),
                (wqa_ref, wqa_in),
                (wka_ref, wka_in),
                (wva_ref, wva_in),
                (wor_ref, wor_in),
                (woa_ref, woa_in),
                (tokens_ref, tokens_in),
                (gain_ref, gain_in),
                (cos_ref, cos_in),
                (sin_ref, sin_in),
                (logs_ref, logs_in),
                (gates_ref, gates_in),
            )
        )
    ]
    all_here = greet(*SP_TP)
    for load in loads:
        load.start()
    for load in loads[:-1]:
        load.wait()
    at = 0
    for ref in (wqr_in, wkr_in, wvr_in, wqa_in, wka_in, wva_in, wor_in, woa_in):
        wall_ref[place + (slice(None), slice(at, at + ref.shape[1]))] = ref[...]
        at += ref.shape[1]
    all_here()
    ring.step(0)
    rows = tokens_in[...].astype(jnp.float32)
    x_ref[x] = (
        rows * lax.rsqrt(jnp.mean(rows * rows, axis=-1, keepdims=True) + EPS) * gain_in[...]
    ).astype(jnp.bfloat16)

    def chunk(slot, k):
        return x_ref.at[lax.rem(slot + 4, 4), :, pl.ds(k * 1024, 1024)]

    def pass_on(slot, k, by, sem):
        remote(chunk(slot, k), chunk(slot, k), x_send, x_recv.at[sem], "tp", by).start()

    pass_on(x, 0, 1, 0)
    pass_on(x, 1, -1, 1)
    pass_on(x, 1, 1, 2)
    pass_on(x, 0, -1, 3)
    ring.step(1)
    columns, _ = running_totals(logs_in[...])
    last = columns[SPAN - 1 : SPAN]
    fade = jnp.exp(per_head(last - columns))
    ring.step(2)
    ring.step(3)
    wait_for(chunk(x - 1, 0), x_recv.at[0])
    pass_on(x - 1, 0, 1, 4)
    wait_for(chunk(x + 1, 1), x_recv.at[1])
    pass_on(x + 1, 1, -1, 5)
    for r in range(4, STEPS):
        ring.step(r)
    wait_for(chunk(x - 1, 1), x_recv.at[2])
    wait_for(chunk(x + 1, 0), x_recv.at[3])
    wait_for(chunk(x - 2, 0), x_recv.at[4])
    wait_for(chunk(x + 2, 1), x_recv.at[5])
    ring.finish()
    sent = x_ref.at[pl.ds(0, 3)]
    wait_for(sent, x_send)

    flat = jnp.dot(
        x_ref[...].reshape(SPAN, 2048),
        wall_ref[:, :, :, :, :IN_WIDTH].reshape(2048, IN_WIDTH),
        preferred_element_type=jnp.float32,
    )
    both = flat[:, : 2 * WIDE]
    lane = lax.rem(lax.broadcasted_iota(jnp.int32, both.shape, 1), HEAD)
    turned = jnp.where(
        lane < HEAD // 2, pltpu.roll(both, 2 * WIDE - HEAD // 2, 1), pltpu.roll(both, HEAD // 2, 1)
    )
    cosine = jnp.concatenate([cos_in[...]] * 3, axis=1)
    sine = jnp.concatenate([sin_in[...]] * 3, axis=1)
    roped = both * cosine + turned * sine
    qr_ref[...] = (roped[:, :WIDE] * HEAD**-0.5).astype(jnp.bfloat16)
    key = roped[:, WIDE:].astype(jnp.bfloat16)
    kr_ref[...] = key
    value = flat[:, 2 * WIDE : 3 * WIDE].astype(jnp.bfloat16)
    vr_ref[...] = value
    faded = (key.astype(jnp.float32) * fade).astype(jnp.bfloat16)
    for h in range(3):
        lanes = slice(h * HEAD, (h + 1) * HEAD)
        update[:, lanes] = lax.dot_general(
            faded[:, lanes],
            value[:, lanes],
            (((0,), (0,)), ((), ())),
            preferred_element_type=jnp.float32,
        )
        query = flat[:, 3 * WIDE + h * HEAD : 3 * WIDE + (h + 1) * HEAD] * (HEAD**-0.5 * LOG2E)
        qa_ref[h * SPAN : (h + 1) * SPAN, :] = jnp.concatenate(
            [query, jnp.zeros_like(query)], axis=1
        ).astype(jnp.bfloat16)
    kvs[place] = flat[:, 4 * WIDE :].astype(jnp.bfloat16)


    ring = SpGather(
        kvs, lambda half: (pl.ds(half * (SPAN // 2), SPAN // 2), slice(None)), sems[4:8]
    )
    prefix = Prefix(states, decays, sems[8:])
    mine = ring.z * 16 + ring.y * 2 + ring.c
    prefix.store(ring.c, (update[...], jnp.broadcast_to(per_head(last), (8, WIDE))))
    acc[...] = jnp.zeros_like(acc)
    tot[...] = jnp.zeros_like(tot)
    for s in range(STEPS + 1):
        prefix.step(s)
        if s < STEPS:
            ring.step(s)
        if s == 1:
            retain_inside(qr_ref, kr_ref, vr_ref, logs_in[...], raw, lifted)
    retain_earlier(raw, lifted, prefix.finish().astype(jnp.bfloat16), wide)
    ring.finish()
    loads[-1].wait()

    def gate_row(block, h, blocks):
        span = pl.ds(pl.multiple_of(block * SPAN, SPAN), blocks * SPAN)
        return gates_in[h : h + 1, span] * LOG2E

    gate_columns = jnp.transpose(
        jnp.concatenate(
            [gate_row(mine, h, 1) for h in range(3)] + [jnp.zeros((5, SPAN), jnp.float32)], axis=0
        )
    )

    def weigh(group, masked):
        keys = kvs[group // 2, pl.ds(lax.rem(group, 2) * 4, 4)].reshape(8 * SPAN, 128)
        for h in range(3):
            rows = pl.ds(h * SPAN, SPAN)
            scores = lax.dot_general(
                qa_ref[rows, :], keys, (((1,), (1,)), ((), ())), preferred_element_type=jnp.float32
            )
            logits = scores + (gate_columns[:, h : h + 1] - gate_row(group * 8, h, 8))
            if masked:
                t = lax.broadcasted_iota(jnp.int32, logits.shape, 0)
                s = lax.broadcasted_iota(jnp.int32, logits.shape, 1)
                logits = jnp.where(s - t <= (mine - group * 8) * SPAN, logits, -jnp.inf)
            weights = jnp.exp2(logits)
            total = weights[:, :128]
            for k in range(1, 16):
                total += weights[:, k * 128 : (k + 1) * 128]
            tot[rows, :] += total
            acc[rows, :] += jnp.dot(
                weights.astype(jnp.bfloat16), keys, preferred_element_type=jnp.float32
            )

    def whole(group, carry):
        weigh(group, False)
        return carry

    lax.fori_loop(0, mine // 8, whole, 0)
    weigh(mine // 8, True)
    for h in range(3):
        rows = pl.ds(h * SPAN, SPAN)
        total = jnp.sum(tot[rows, :], axis=1, keepdims=True)
        wide[:, WIDE + h * HEAD : WIDE + (h + 1) * HEAD] = (acc[rows, HEAD:] / total).astype(
            jnp.bfloat16
        )

    def columns(k):
        return pl.ds(k * 512, 512)

    for k in range(4):
        weights = wall_ref[2 * k : 2 * k + 2, :, :, :, IN_WIDTH:].reshape(512, 2 * WIDE)
        part[:, :, k * 512 : (k + 1) * 512] = (
            lax.dot_general(
                wide[...], weights, (((1,), (1,)), ((), ())), preferred_element_type=jnp.float32
            )
            .astype(jnp.bfloat16)
            .reshape(4, SPAN // 4, 512)
        )
        for by in (2, 1, 3):
            remote(
                part.at[lax.rem(x + by, 4), :, columns(k)],
                inbox.at[by - 1, :, columns(k)],
                out_send,
                out_recv.at[by - 1, k],
                "tp",
                by,
            ).start()
    for k in range(4):
        total = part[x, :, k * 512 : (k + 1) * 512].astype(jnp.float32)
        for by in (1, 3, 2):
            wait_for(inbox.at[by - 1, :, columns(k)], out_recv.at[by - 1, k])
            total += inbox[by - 1, :, k * 512 : (k + 1) * 512].astype(jnp.float32)
        out_ref[:, k * 512 : (k + 1) * 512] = total.astype(jnp.bfloat16)
    wait_for(inbox, out_send)


def layer(*operands):
    bf16, f32 = jnp.bfloat16, jnp.float32
    return pl.pallas_call(
        layer_kernel,
        out_shape=jax.ShapeDtypeStruct((SPAN // 4, 2048), bf16),
        in_specs=[ANY] * len(operands),
        out_specs=VMEM,
        scratch_shapes=[
            *(pltpu.VMEM(a.shape, a.dtype) for a in operands),
            pltpu.VMEM((8, 8, 2, 16, ALL_WIDTH), bf16),
            pltpu.VMEM((4, 64, 2048), bf16),
            pltpu.VMEM((SPAN, WIDE), bf16),
            pltpu.VMEM((SPAN, WIDE), bf16),
            pltpu.VMEM((SPAN, WIDE), bf16),
            pltpu.VMEM((3 * SPAN, 128), bf16),
            pltpu.VMEM((HEAD, WIDE), f32),
            pltpu.VMEM((8, 8, 2, SPAN, 128), bf16),
            pltpu.VMEM((18, HEAD, WIDE), bf16),
            pltpu.VMEM((18, 8, WIDE), f32),
            pltpu.VMEM((3 * SPAN, 128), f32),
            pltpu.VMEM((3 * SPAN, 128), f32),
            pltpu.VMEM((SPAN, WIDE), f32),
            pltpu.VMEM((SPAN, WIDE), bf16),
            pltpu.VMEM((SPAN, 2 * WIDE), bf16),
            pltpu.VMEM((4, SPAN // 4, 2048), bf16),
            pltpu.VMEM((3, SPAN // 4, 2048), bf16),
            pltpu.SemaphoreType.DMA((len(operands),)),
            pltpu.SemaphoreType.DMA,
            pltpu.SemaphoreType.DMA((6,)),
            pltpu.SemaphoreType.DMA,
            pltpu.SemaphoreType.DMA((3, 4)),
            *GATHER_SEMS,
            *GATHER_SEMS,
            *PREFIX_SEMS,
        ],
        compiler_params=pltpu.CompilerParams(
            collective_id=1, has_side_effects=True, vmem_limit_bytes=60 * 2**20
        ),
    )(*operands)


def angles_of(positions):
    half = HEAD // 2
    inverse = THETA ** (-jnp.arange(half, dtype=jnp.float32) / half)
    return positions[:, None] * inverse[None, :]


def body(
    tokens,
    pre_gain,
    w_query_ret,
    w_key_ret,
    w_value_ret,
    w_query_att,
    w_key_att,
    w_value_att,
    w_out_ret,
    w_out_att,
    retain_log,
    forget_total,
):
    offset = lax.axis_index(SP) * SPAN
    positions = (offset + jnp.arange(SPAN, dtype=jnp.int32)).astype(jnp.float32)
    angles = angles_of(positions)
    cosine, sine = jnp.cos(angles), jnp.sin(angles)
    cosine = jnp.concatenate([cosine] * 4, axis=1)
    sine = jnp.concatenate([-sine, sine] * 2, axis=1)
    return layer(
        tokens,
        pre_gain.reshape(1, -1),
        w_query_ret,
        w_key_ret,
        w_value_ret,
        w_query_att,
        w_key_att,
        w_value_att,
        w_out_ret.T,
        w_out_att.T,
        cosine,
        sine,
        retain_log.T,
        forget_total,
    )


def solution(mesh):
    finer = Mesh(mesh.devices.reshape(8, 8, 2, mesh.shape["tp"]), ("sp_0", "sp_1", "sp_2", "tp"))
    placed = (
        P(SP_TP, None),
        P(),
        P(SP, "tp"),
        P(SP, "tp"),
        P(SP, "tp"),
        P(SP, "tp"),
        P(SP, "tp"),
        P(SP, "tp"),
        P("tp", SP),
        P("tp", SP),
        P(SP, "tp"),
        P("tp", None),
    )
    return jax.shard_map(
        body, mesh=finer, in_specs=placed, out_specs=P(SP_TP, None), check_vma=False
    )
```

time: 175 us -> 125 us (0.71)
  Pallas kernels: 141 us -> 121 us
  blocking collectives: 19 us -> 0 us
  local copies, waits for them, and re-layouts: 12.5 us -> 1.67 us
    pallas_call x3 -> x1, Pallas kernels: 141 us -> 121 us  [layer(): pl.pallas_call(layer_kernel, out_shape=jax.ShapeDtypeStruct((SPAN // 4, 2...]
    all_to_all x1 -> x0, blocking collectives: 19 us -> none  [sent_and_summed(): lax.all_to_all(cut_along(shard, dim, devices), axis, 0, 0, tiled=True)]
    unnamed x23 -> x1, local copies, waits for them, and re-layouts: 12.5 us -> 1.67 us
where the time goes in v2:
time: 125 us; the launch traced here: 124 us
  Pallas kernels  121 us (97%)
  local copies, waits for them, and re-layouts  1.67 us (1%)
  other arithmetic  1.53 us (1%)
    pallas_call x1, Pallas kernels, layer(): pl.pallas_call(layer_kernel, out_shape=jax.ShapeDtypeStruct((SPAN // 4, 2...  121 us

profile of v2, /device:TPU:504, one launch (start us, length us, event | category | flops | bytes accessed | tf_op | source)
XLA Modules:
  0.0 124.5 jit_solution(1185678720191524076)
XLA Ops:
  0.0 0.5 fusion
  0.6 1.0 pad_maximum_fusion
  1.5 121.3 %shard_map.118 = bf16[64,2048]{1,0:T(8,128)(2,1)} custom-call(bf16[64,2048]{1,0:T(8,128)(2,1)} %tokens_ref.1, f32[1,2048]{1,0:T(1,128)} %bitcast.4, bf16[16,192]{1,0:T(8,128)(2,1)} %wqr_ref.1, bf16[16,192]{1,0:T(8,128)(2,1)} %wkr_ref.1, bf16[16,192]{1,0:T(8,128)(2,1)} %wvr_ref.1, bf16[16,192]{1,0:T(8,128)(2,1)} %wqa_ref.1, bf16[16,64]{1,0:T(8,128)(2,1)} %wka_ref.1, ...), custom_call_target="tpu_custom_call" | custom-call | tf_op jit(solution)/shard_map/pallas_call | solution.py:559
  122.8 1.7 %copy.15 = bf16[64,2048]{1,0:T(8,128)(2,1)} copy(bf16[64,2048]{1,0:T(8,128)(2,1)} %shard_map.118) | data formatting | bytes 524288
  (2 shorter events, 0.0 us)

commit v3 on v2

--- a/solution.py
+++ b/solution.py
@@ -77,8 +77,8 @@
 
 
 class SpGather:
-    def __init__(self, ref, part, sems):
-        self.ref, self.part = ref, part
+    def __init__(self, ref, part, sems, by_piece=False):
+        self.ref, self.part, self.by_piece = ref, part, by_piece
         self.send_sem, self.recv_sem, self.swap_send, self.swap_recv = sems
         self.z, self.y, self.c = (lax.axis_index(a) for a in SP)
 
@@ -102,8 +102,34 @@
         wait_for(ref, self.recv_sem.at[half, SLOTS[slot]])
 
     def swap(self, half, second):
+        if self.by_piece:
+            return
         ref = self.slab(half, second)
         remote(ref, ref, self.swap_send.at[half], self.swap_recv.at[half], "sp_2", 1).start()
+
+    def swap_pieces(self, s):
+        for half in (0, 1):
+            a, b = self.coords(half)
+            for delta in DELTAS:
+                for delta_2 in DELTAS:
+                    if abs(delta) + abs(delta_2) == s:
+                        ref = self.piece(half, ring_index(a - delta), ring_index(b - delta_2))
+                        remote(
+                            ref,
+                            ref,
+                            self.swap_send.at[half],
+                            self.swap_recv.at[half, s],
+                            "sp_2",
+                            1,
+                        ).start()
+
+    def wait_swapped(self, s):
+        rows, columns = ((1, 1), (2, 2), (1, 8), (2, 6), (2, 7), (2, 6), (1, 8), (2, 2), (1, 1))[s]
+        for half in (0, 1):
+            wait_for(
+                self.ref.at[(slice(0, rows), slice(0, columns), 0) + self.part(half)],
+                self.swap_recv.at[half, s],
+            )
 
     def step(self, s):
         for half in (0, 1):
@@ -142,7 +168,8 @@
     def finish(self):
         for half in (0, 1):
             core = self.ref.at[(slice(None), slice(None), 0) + self.part(half)]
-            wait_for(core, self.swap_recv.at[half])
+            if not self.by_piece:
+                wait_for(core, self.swap_recv.at[half])
             wait_for(core, self.swap_send.at[half])
             wait_for(
                 self.ref.at[(slice(0, 7), slice(None), 0) + self.part(half)],
@@ -463,60 +490,97 @@
 
 
     ring = SpGather(
-        kvs, lambda half: (pl.ds(half * (SPAN // 2), SPAN // 2), slice(None)), sems[4:8]
+        kvs, lambda half: (pl.ds(half * (SPAN // 2), SPAN // 2), slice(None)), sems[4:8], True
     )
     prefix = Prefix(states, decays, sems[8:])
     mine = ring.z * 16 + ring.y * 2 + ring.c
     prefix.store(ring.c, (update[...], jnp.broadcast_to(per_head(last), (8, WIDE))))
     acc[...] = jnp.zeros_like(acc)
     tot[...] = jnp.zeros_like(tot)
+    def gate_row(block, h):
+        return gates_in[h : h + 1, pl.ds(pl.multiple_of(block * SPAN, SPAN), SPAN)] * LOG2E
+
+    loads[-1].wait()
+    gate_columns = jnp.transpose(
+        jnp.concatenate(
+            [gate_row(mine, h) for h in range(3)] + [jnp.zeros((5, SPAN), jnp.float32)], axis=0
+        )
+    )
+
+    def weigh(places, own_first=False):
+        blocks = [z * 16 + y * 2 + c for z, y, c in places]
+        limits = [mine + (1 if own_first and k == 0 else 0) for k in range(4)]
+        allowed = [block < limit for block, limit in zip(blocks, limits)]
+
+        def add():
+            keys = jnp.concatenate([kvs[place] for place in places], axis=0)
+            for h in range(3):
+                rows = pl.ds(h * SPAN, SPAN)
+                scores = lax.dot_general(
+                    qa_ref[rows, :],
+                    keys,
+                    (((1,), (1,)), ((), ())),
+                    preferred_element_type=jnp.float32,
+                )
+                fall = jnp.concatenate(
+                    [
+                        jnp.where(block < limit, gate_row(block, h), jnp.inf)
+                        for block, limit in zip(blocks, limits)
+                    ],
+                    axis=1,
+                )
+                logits = scores + (gate_columns[:, h : h + 1] - fall)
+                if own_first:
+                    t = lax.broadcasted_iota(jnp.int32, logits.shape, 0)
+                    at = lax.broadcasted_iota(jnp.int32, logits.shape, 1)
+                    logits = jnp.where((at >= SPAN) | (at <= t), logits, -jnp.inf)
+                weights = jnp.exp2(logits)
+                total = weights[:, :128]
+                for k in range(1, 8):
+                    total += weights[:, k * 128 : (k + 1) * 128]
+                tot[rows, :] += total
+                acc[rows, :] += jnp.dot(
+                    weights.astype(jnp.bfloat16), keys, preferred_element_type=jnp.float32
+                )
+
+        if own_first:
+            add()
+        else:
+            pl.when(allowed[0] | allowed[1] | allowed[2] | allowed[3])(add)
+
+    def at_offset(down, across, core):
+        return ring_index(ring.z + down), ring_index(ring.y + across), core
+
+    def weigh_distance(distance):
+        low, high = max(1, distance - 4), min(3, distance)
+
+        def turns(index, carry):
+            q = low + index // 2
+            p, core = distance - q, lax.rem(index, 2)
+            weigh([at_offset(*off, core) for off in ((p, q), (-q, p), (-p, -q), (q, -p))])
+            return carry
+
+        lax.fori_loop(0, 2 * (high - low + 1), turns, 0)
+
     for s in range(STEPS + 1):
         prefix.step(s)
         if s < STEPS:
             ring.step(s)
+            ring.swap_pieces(s)
         if s == 1:
             retain_inside(qr_ref, kr_ref, vr_ref, logs_in[...], raw, lifted)
+        if s >= 1:
+            ring.wait_swapped(s - 1)
+        if 2 <= s <= 8:
+            weigh_distance(s - 1)
+        if s == 8:
+            weigh([at_offset(*off, core) for off in ((0, 4), (4, 0)) for core in (0, 1)])
+    weigh(
+        [at_offset(*off, core) for off in ((0, 0), (4, 4)) for core in (ring.c, 1 - ring.c)],
+        own_first=True,
+    )
     retain_earlier(raw, lifted, prefix.finish().astype(jnp.bfloat16), wide)
     ring.finish()
-    loads[-1].wait()
-
-    def gate_row(block, h, blocks):
-        span = pl.ds(pl.multiple_of(block * SPAN, SPAN), blocks * SPAN)
-        return gates_in[h : h + 1, span] * LOG2E
-
-    gate_columns = jnp.transpose(
-        jnp.concatenate(
-            [gate_row(mine, h, 1) for h in range(3)] + [jnp.zeros((5, SPAN), jnp.float32)], axis=0
-        )
-    )
-
-    def weigh(group, masked):
-        keys = kvs[group // 2, pl.ds(lax.rem(group, 2) * 4, 4)].reshape(8 * SPAN, 128)
-        for h in range(3):
-            rows = pl.ds(h * SPAN, SPAN)
-            scores = lax.dot_general(
-                qa_ref[rows, :], keys, (((1,), (1,)), ((), ())), preferred_element_type=jnp.float32
-            )
-            logits = scores + (gate_columns[:, h : h + 1] - gate_row(group * 8, h, 8))
-            if masked:
-                t = lax.broadcasted_iota(jnp.int32, logits.shape, 0)
-                s = lax.broadcasted_iota(jnp.int32, logits.shape, 1)
-                logits = jnp.where(s - t <= (mine - group * 8) * SPAN, logits, -jnp.inf)
-            weights = jnp.exp2(logits)
-            total = weights[:, :128]
-            for k in range(1, 16):
-                total += weights[:, k * 128 : (k + 1) * 128]
-            tot[rows, :] += total
-            acc[rows, :] += jnp.dot(
-                weights.astype(jnp.bfloat16), keys, preferred_element_type=jnp.float32
-            )
-
-    def whole(group, carry):
-        weigh(group, False)
-        return carry
-
-    lax.fori_loop(0, mine // 8, whole, 0)
-    weigh(mine // 8, True)
     for h in range(3):
         rows = pl.ds(h * SPAN, SPAN)
         total = jnp.sum(tot[rows, :], axis=1, keepdims=True)
@@ -586,7 +650,8 @@
             pltpu.SemaphoreType.DMA,
             pltpu.SemaphoreType.DMA((3, 4)),
             *GATHER_SEMS,
-            *GATHER_SEMS,
+            *GATHER_SEMS[:3],
+            pltpu.SemaphoreType.DMA((2, STEPS)),
             *PREFIX_SEMS,
         ],
         compiler_params=pltpu.CompilerParams(

time: 125 us -> 113 us (0.904)
  the two profiles are of different devices: /device:TPU:504 before, /device:TPU:8 now
where the time goes in v3:
time: 113 us
  Pallas kernels  110 us (97%)
  local copies, waits for them, and re-layouts  1.67 us (1%)
  other arithmetic  1.53 us (1%)
    pallas_call x1, Pallas kernels, layer(): pl.pallas_call(layer_kernel, out_shape=jax.ShapeDtypeStruct((SPAN // 4, 2...  110 us

profile of v3, /device:TPU:8, one launch (start us, length us, event | category | flops | bytes accessed | tf_op | source)
XLA Modules:
  0.0 112.9 jit_solution(3641287662397327480)
XLA Ops:
  0.0 0.5 fusion
  0.6 1.0 pad_maximum_fusion
  1.5 109.7 %shard_map.118 = bf16[64,2048]{1,0:T(8,128)(2,1)} custom-call(bf16[64,2048]{1,0:T(8,128)(2,1)} %tokens_ref.1, f32[1,2048]{1,0:T(1,128)} %bitcast.4, bf16[16,192]{1,0:T(8,128)(2,1)} %wqr_ref.1, bf16[16,192]{1,0:T(8,128)(2,1)} %wkr_ref.1, bf16[16,192]{1,0:T(8,128)(2,1)} %wvr_ref.1, bf16[16,192]{1,0:T(8,128)(2,1)} %wqa_ref.1, bf16[16,64]{1,0:T(8,128)(2,1)} %wka_ref.1, ...), custom_call_target="tpu_custom_call" | custom-call | tf_op jit(solution)/shard_map/pallas_call | solution.py:623
  111.2 1.7 %copy.15 = bf16[64,2048]{1,0:T(8,128)(2,1)} copy(bf16[64,2048]{1,0:T(8,128)(2,1)} %shard_map.118) | data formatting | bytes 524288
  (2 shorter events, 0.0 us)

commit v4 on v3

--- a/solution.py
+++ b/solution.py
@@ -132,38 +132,46 @@
             )
 
     def step(self, s):
+        for delta in sorted({s, -s}, reverse=True):
+            if delta in DELTAS:
+                for half in (0, 1):
+                    self.enter(half, delta)
+        for k in range(4):
+            for delta in DELTAS:
+                if abs(delta) != s - 1 - k:
+                    continue
+                for by in (1, -1):
+                    for half in (0, 1):
+                        if (by, delta, k) in SLOTS:
+                            self.pass_along(half, by, delta, k)
         for half in (0, 1):
-            a, b = self.coords(half)
-            first, second = ("sp_1", "sp_0") if half == 0 else ("sp_0", "sp_1")
-            for delta in sorted({s, -s}, reverse=True):
-                if delta not in DELTAS:
-                    continue
-                ref = self.piece(half, ring_index(a - delta), b)
-                if delta:
-                    self.arrived(half, ref, ("first", delta))
-                for further in (1, -1) if delta == 0 else (delta + (1 if delta > 0 else -1),):
-                    if further in DELTAS:
-                        self.send(half, ref, first, 1 if further > 0 else -1, ("first", further))
-                for by in (1, -1):
-                    self.send(half, ref, second, by, (by, delta, 0))
+            b = self.coords(half)[1]
             if s == 4:
                 self.swap(half, b)
-            for k in range(4):
-                for delta in DELTAS:
-                    if abs(delta) != s - 1 - k:
-                        continue
-                    for by in (1, -1):
-                        if (by, delta, k) not in SLOTS:
-                            continue
-                        ref = self.piece(half, ring_index(a - delta), ring_index(b - by * (k + 1)))
-                        self.arrived(half, ref, (by, delta, k))
-                        if (by, delta, k + 1) in SLOTS:
-                            self.send(half, ref, second, by, (by, delta, k + 1))
             if 5 <= s < 8:
                 self.swap(half, ring_index(b - (s - 4)))
                 self.swap(half, ring_index(b + (s - 4)))
             if s == 8:
                 self.swap(half, ring_index(b + 4))
+
+    def enter(self, half, delta):
+        a, b = self.coords(half)
+        first, second = ("sp_1", "sp_0") if half == 0 else ("sp_0", "sp_1")
+        ref = self.piece(half, ring_index(a - delta), b)
+        if delta:
+            self.arrived(half, ref, ("first", delta))
+        for further in (1, -1) if delta == 0 else (delta + (1 if delta > 0 else -1),):
+            if further in DELTAS:
+                self.send(half, ref, first, 1 if further > 0 else -1, ("first", further))
+        for by in (1, -1):
+            self.send(half, ref, second, by, (by, delta, 0))
+
+    def pass_along(self, half, by, delta, k):
+        a, b = self.coords(half)
+        ref = self.piece(half, ring_index(a - delta), ring_index(b - by * (k + 1)))
+        self.arrived(half, ref, (by, delta, k))
+        if (by, delta, k + 1) in SLOTS:
+            self.send(half, ref, "sp_0" if half == 0 else "sp_1", by, (by, delta, k + 1))
 
     def finish(self):
         for half in (0, 1):
@@ -184,7 +192,7 @@
     pltpu.SemaphoreType.DMA((2,)),
     pltpu.SemaphoreType.DMA((2, len(SLOTS))),
     pltpu.SemaphoreType.DMA((2,)),
-    pltpu.SemaphoreType.DMA((2,)),
+    pltpu.SemaphoreType.DMA((2, STEPS)),
 ]
 
 
@@ -384,7 +392,7 @@
 ):
     half_width = ALL_WIDTH // 2
     ring = SpGather(
-        wall_ref, lambda half: (slice(None), pl.ds(half * half_width, half_width)), sems[:4]
+        wall_ref, lambda half: (slice(None), pl.ds(half * half_width, half_width)), sems[:4], True
     )
     x = lax.axis_index("tp")
     place = (ring.z, ring.y, ring.c)
@@ -435,22 +443,28 @@
     pass_on(x, 1, -1, 1)
     pass_on(x, 1, 1, 2)
     pass_on(x, 0, -1, 3)
+    ring.swap_pieces(0)
     ring.step(1)
+    ring.swap_pieces(1)
     columns, _ = running_totals(logs_in[...])
     last = columns[SPAN - 1 : SPAN]
     fade = jnp.exp(per_head(last - columns))
-    ring.step(2)
-    ring.step(3)
+    for r in (2, 3):
+        ring.step(r)
+        ring.swap_pieces(r)
     wait_for(chunk(x - 1, 0), x_recv.at[0])
     pass_on(x - 1, 0, 1, 4)
     wait_for(chunk(x + 1, 1), x_recv.at[1])
     pass_on(x + 1, 1, -1, 5)
     for r in range(4, STEPS):
         ring.step(r)
+        ring.swap_pieces(r)
     wait_for(chunk(x - 1, 1), x_recv.at[2])
     wait_for(chunk(x + 1, 0), x_recv.at[3])
     wait_for(chunk(x - 2, 0), x_recv.at[4])
     wait_for(chunk(x + 2, 1), x_recv.at[5])
+    for r in range(STEPS):
+        ring.wait_swapped(r)
     ring.finish()
     sent = x_ref.at[pl.ds(0, 3)]
     wait_for(sent, x_send)
@@ -551,16 +565,16 @@
     def at_offset(down, across, core):
         return ring_index(ring.z + down), ring_index(ring.y + across), core
 
-    def weigh_distance(distance):
+    def weigh_distance(distance, core):
         low, high = max(1, distance - 4), min(3, distance)
 
         def turns(index, carry):
-            q = low + index // 2
-            p, core = distance - q, lax.rem(index, 2)
+            q = low + index
+            p = distance - q
             weigh([at_offset(*off, core) for off in ((p, q), (-q, p), (-p, -q), (q, -p))])
             return carry
 
-        lax.fori_loop(0, 2 * (high - low + 1), turns, 0)
+        lax.fori_loop(0, high - low + 1, turns, 0)
 
     for s in range(STEPS + 1):
         prefix.step(s)
@@ -569,10 +583,12 @@
             ring.swap_pieces(s)
         if s == 1:
             retain_inside(qr_ref, kr_ref, vr_ref, logs_in[...], raw, lifted)
+        if 1 <= s <= 7:
+            weigh_distance(s, ring.c)
         if s >= 1:
             ring.wait_swapped(s - 1)
         if 2 <= s <= 8:
-            weigh_distance(s - 1)
+            weigh_distance(s - 1, 1 - ring.c)
         if s == 8:
             weigh([at_offset(*off, core) for off in ((0, 4), (4, 0)) for core in (0, 1)])
     weigh(
@@ -650,8 +666,7 @@
             pltpu.SemaphoreType.DMA,
             pltpu.SemaphoreType.DMA((3, 4)),
             *GATHER_SEMS,
-            *GATHER_SEMS[:3],
-            pltpu.SemaphoreType.DMA((2, STEPS)),
+            *GATHER_SEMS,
             *PREFIX_SEMS,
         ],
         compiler_params=pltpu.CompilerParams(

time: 113 us -> 110 us (0.973)
  Pallas kernels: 110 us -> 106 us
    pallas_call x1, Pallas kernels: 110 us -> 106 us  [layer(): pl.pallas_call(layer_kernel, out_shape=jax.ShapeDtypeStruct((SPAN // 4, 2...]
where the time goes in v4:
time: 110 us
  Pallas kernels  106 us (96%)
  local copies, waits for them, and re-layouts  1.67 us (2%)
  other arithmetic  1.53 us (1%)
    pallas_call x1, Pallas kernels, layer(): pl.pallas_call(layer_kernel, out_shape=jax.ShapeDtypeStruct((SPAN // 4, 2...  106 us

profile of v4, /device:TPU:8, one launch (start us, length us, event | category | flops | bytes accessed | tf_op | source)
XLA Modules:
  0.0 109.7 jit_solution(970743337218126903)
XLA Ops:
  0.0 0.5 fusion
  0.6 1.0 pad_maximum_fusion
  1.5 106.4 %shard_map.118 = bf16[64,2048]{1,0:T(8,128)(2,1)} custom-call(bf16[64,2048]{1,0:T(8,128)(2,1)} %tokens_ref.1, f32[1,2048]{1,0:T(1,128)} %bitcast.4, bf16[16,192]{1,0:T(8,128)(2,1)} %wqr_ref.1, bf16[16,192]{1,0:T(8,128)(2,1)} %wkr_ref.1, bf16[16,192]{1,0:T(8,128)(2,1)} %wvr_ref.1, bf16[16,192]{1,0:T(8,128)(2,1)} %wqa_ref.1, bf16[16,64]{1,0:T(8,128)(2,1)} %wka_ref.1, ...), custom_call_target="tpu_custom_call" | custom-call | tf_op jit(solution)/shard_map/pallas_call | solution.py:639
  108.0 1.7 %copy.15 = bf16[64,2048]{1,0:T(8,128)(2,1)} copy(bf16[64,2048]{1,0:T(8,128)(2,1)} %shard_map.118) | data formatting | bytes 524288
  (2 shorter events, 0.0 us)
